TPU v7x, 32 devices: a whole 2x2x4 slice. The times are simulated.
32 devices in a mesh: sp: 8 (over z, x), tp: 4 (over y, core).
Axes of the slice: x: 2, y: 2, z: 4, core: 2. Of those that a mesh axis runs over, the one named last changes fastest.
Arguments:
- upstream: bfloat16 [2048, 2048], P('sp'), may hold values from -6 to 6
- stream: bfloat16 [2048, 2048], P('sp'), may hold values from -10 to 10
- routes: int32 [2048, 2], P('sp'), may hold values from 0 to 7, all different within a row; in each aligned block of 256 rows (0 to 255, 256 to 511, ...) at most 128 rows name the same one
- route_weights: float32 [2048, 2], P('sp'), may hold values from 0.1 to 1
- glu_value: bfloat16 [2048, 512], P('sp', 'tp'), may hold values from -6 to 6
- glu_gate: bfloat16 [2048, 512], P('sp', 'tp'), may hold values from -10 to 10
- conv_taps: float32 [31, 512], P(None, 'tp'), may hold values from -1 to 1
- conv_saved: bfloat16 [2048, 512], P('sp', 'tp'), may hold values from -600 to 600
- out_proj: bfloat16 [2048, 512], P(None, 'tp'), may hold values from -0.25 to 0.25
- expert_gate: bfloat16 [8, 2048, 2048], P('sp', None, 'tp'), may hold values from -0.125 to 0.125
- expert_up: bfloat16 [8, 2048, 2048], P('sp', None, 'tp'), may hold values from -0.125 to 0.125
- expert_down: bfloat16 [8, 2048, 2048], P('sp', 'tp'), may hold values from -0.125 to 0.125
Outputs:
- grad_stream: bfloat16 [2048, 2048], P('sp', 'tp')
- grad_value: bfloat16 [2048, 512], P('sp', 'tp')
- grad_gate: bfloat16 [2048, 512], P('sp', 'tp')
- grad_out_proj: float32 [2048, 512], P('sp', 'tp')
- grad_expert_gate: float32 [8, 2048, 2048], P('sp', None, 'tp')
- grad_expert_up: float32 [8, 2048, 2048], P('sp', None, 'tp')
- grad_expert_down: float32 [8, 2048, 2048], P('sp', 'tp')
Inputs may be any that keep to these rules, and one draw needn't show every extreme that they name: `routes`: each row names 2 different experts; among the 256 rows of one index of sp no expert is named more than 128 times, a bound that some block reaches.
All inputs are finite; a program needn't handle non-finite values.
Results may differ from a plain program's by a relative error of at most 0.014.
Values may be sent and summed in bfloat16 or wider, within the bound.
A program may use at most 128 MiB of HBM per device.

v0:
```python
import jax
import jax.numpy as jnp
from jax import lax
from jax.sharding import PartitionSpec as P

CW = 512


clamp_limit = 7.0
glu_alpha = 1.702
norm_eps = 1e-05


def passed_along(shard, axis, by):
    size = lax.axis_size(axis)
    pairs = [(i, i + by) for i in range(size) if 0 <= i + by < size]
    return lax.ppermute(shard, axis, pairs)


def contract_rows(left, right):
    return lax.dot_general(
        left, right, (((0,), (0,)), ((), ())), preferred_element_type=jnp.float32
    )


def times_transposed(left, right):
    return lax.dot_general(
        left, right, (((1,), (1,)), ((), ())), preferred_element_type=jnp.float32
    )


def block_slots(block_routes, expert_count, capacity):
    flat_routes = block_routes.reshape(-1)
    one_hot = (flat_routes[:, None] == jnp.arange(expert_count, dtype=jnp.int32)[None, :]).astype(
        jnp.int32
    )
    earlier = jnp.cumsum(one_hot, axis=0) - one_hot
    slot_index = jnp.sum(earlier * one_hot, axis=1)
    target = flat_routes * capacity + slot_index
    pair_count = flat_routes.shape[0]
    table = (
        jnp.full((expert_count * capacity,), pair_count, jnp.int32)
        .at[target]
        .set(jnp.arange(pair_count, dtype=jnp.int32))
    )
    return (target, table)


def gather_pairs(table, block_stream, block_upstream, block_weights, topk):
    token_of = table // topk
    zero_row = jnp.zeros((1, block_stream.shape[1]), jnp.bfloat16)
    stream_pad = jnp.concatenate([block_stream, zero_row], axis=0)
    upstream_pad = jnp.concatenate([block_upstream, zero_row], axis=0)
    weight_pad = jnp.concatenate([block_weights.reshape(-1), jnp.zeros((1,), jnp.float32)])
    send_rows = stream_pad[token_of]
    send_cot = (weight_pad[table][:, None] * upstream_pad[token_of].astype(jnp.float32)).astype(
        jnp.bfloat16
    )
    return (send_rows, send_cot)


def expert_backward(expert_rows, expert_cot, gate_weight, up_weight, down_weight):
    gate_pre = jnp.dot(expert_rows, gate_weight, preferred_element_type=jnp.float32)
    up_pre = jnp.dot(expert_rows, up_weight, preferred_element_type=jnp.float32)
    capped = jnp.minimum(gate_pre, clamp_limit)
    clipped = jnp.clip(up_pre, -clamp_limit, clamp_limit)
    gate_sigmoid = jax.nn.sigmoid(glu_alpha * capped)
    act = (capped * gate_sigmoid * (clipped + 1.0)).astype(jnp.bfloat16)
    grad_down = contract_rows(act, expert_cot)
    grad_act = times_transposed(expert_cot, down_weight)
    slope = gate_sigmoid + glu_alpha * capped * gate_sigmoid * (1.0 - gate_sigmoid)
    grad_gate_pre = jnp.where(
        gate_pre < clamp_limit, grad_act * (clipped + 1.0) * slope, 0.0
    ).astype(jnp.bfloat16)
    grad_up_pre = jnp.where(
        jnp.abs(up_pre) < clamp_limit, grad_act * capped * gate_sigmoid, 0.0
    ).astype(jnp.bfloat16)
    grad_gate = contract_rows(expert_rows, grad_gate_pre)
    grad_up = contract_rows(expert_rows, grad_up_pre)
    return (grad_gate, grad_up, grad_down, grad_gate_pre, grad_up_pre)


def on_device(
    upstream,
    stream,
    routes,
    route_weights,
    glu_value,
    glu_gate,
    conv_taps,
    conv_saved,
    out_proj,
    expert_gate,
    expert_up,
    expert_down,
):
    tok_count = upstream.shape[0]
    model_width = upstream.shape[1]
    topk = routes.shape[1]
    expert_count = lax.axis_size("sp")
    capacity = 4 * tok_count // expert_count
    slice_width = model_width // lax.axis_size("tp")
    column_start = lax.axis_index("tp") * slice_width
    target, table = block_slots(routes, expert_count, capacity)
    stream_part = lax.dynamic_slice_in_dim(stream, column_start, slice_width, 1)
    upstream_part = lax.dynamic_slice_in_dim(upstream, column_start, slice_width, 1)
    send_rows, send_cot = gather_pairs(table, stream_part, upstream_part, route_weights, topk)
    part_shape = (expert_count, capacity, slice_width)
    part_rows, part_cot = (
        lax.all_to_all(
            send_rows.reshape(part_shape), "sp", split_axis=0, concat_axis=0, tiled=True
        ),
        lax.all_to_all(send_cot.reshape(part_shape), "sp", split_axis=0, concat_axis=0, tiled=True),
    )
    got_rows, got_cot = (
        lax.all_gather(part_rows, "tp", axis=2, tiled=True),
        lax.all_gather(part_cot, "tp", axis=2, tiled=True),
    )
    expert_rows = got_rows.reshape(-1, model_width)
    expert_cot = got_cot.reshape(-1, model_width)
    gate_weight = expert_gate[0]
    up_weight = expert_up[0]
    down_weight = expert_down[0]
    grad_gate_w, grad_up_w, grad_down_w, grad_gate_pre, grad_up_pre = expert_backward(
        expert_rows, expert_cot, gate_weight, up_weight, down_weight
    )
    partial_rows = times_transposed(grad_gate_pre, gate_weight) + times_transposed(
        grad_up_pre, up_weight
    )
    summed_rows = lax.psum_scatter(
        partial_rows.astype(jnp.bfloat16), "tp", scatter_dimension=1, tiled=True
    )
    returned = lax.all_to_all(
        summed_rows.reshape(expert_count, capacity, slice_width),
        "sp",
        split_axis=0,
        concat_axis=0,
        tiled=True,
    )
    pair_grads = returned.reshape(expert_count * capacity, slice_width)[target].astype(jnp.float32)
    routed_sum = jnp.sum(pair_grads.reshape(tok_count, topk, slice_width), axis=1)
    upstream_own = lax.dynamic_slice_in_dim(upstream, column_start, slice_width, 1)
    grad_stream = (upstream_own.astype(jnp.float32) + routed_sum).astype(jnp.bfloat16)
    full_grad = lax.all_gather(grad_stream, "tp", axis=1, tiled=True)
    saved_conv = conv_saved.astype(jnp.float32)
    total_sum, square_sum = lax.psum(
        (jnp.sum(saved_conv, axis=1), jnp.sum(saved_conv * saved_conv, axis=1)), "tp"
    )
    mean_c = (total_sum / CW)[:, None]
    var_c = (square_sum / CW)[:, None] - mean_c * mean_c
    inv_std = lax.rsqrt(var_c + norm_eps)
    normed = (saved_conv - mean_c) * inv_std
    norm_sigmoid = jax.nn.sigmoid(normed)
    mixed = (normed * norm_sigmoid).astype(jnp.bfloat16)
    grad_mixed = jnp.dot(full_grad, out_proj, preferred_element_type=jnp.float32)
    grad_normed = grad_mixed * norm_sigmoid * (1.0 + normed * (1.0 - norm_sigmoid))
    first_sum, second_sum = lax.psum(
        (jnp.sum(grad_normed, axis=1), jnp.sum(grad_normed * normed, axis=1)), "tp"
    )
    grad_conv = inv_std * (
        grad_normed - (first_sum / CW)[:, None] - normed * (second_sum / CW)[:, None]
    )
    kernel_width = conv_taps.shape[0]
    rim_rows = passed_along(grad_conv[: kernel_width - 1], "sp", -1)
    padded = jnp.concatenate([grad_conv, rim_rows], axis=0)
    grad_glu = jnp.zeros_like(grad_conv)
    for offset in range(kernel_width):
        grad_glu = grad_glu + conv_taps[offset][None, :] * padded[offset : offset + tok_count]
    gate_sig = jax.nn.sigmoid(glu_gate.astype(jnp.float32))
    grad_value = (grad_glu * gate_sig).astype(jnp.bfloat16)
    grad_gate = (grad_glu * glu_value.astype(jnp.float32) * gate_sig * (1.0 - gate_sig)).astype(
        jnp.bfloat16
    )
    grad_out_proj = lax.psum_scatter(
        contract_rows(full_grad, mixed), "sp", scatter_dimension=0, tiled=True
    )
    return (
        grad_stream,
        grad_value,
        grad_gate,
        grad_out_proj,
        grad_gate_w[None],
        grad_up_w[None],
        grad_down_w[None],
    )


def solution(mesh):
    in_specs = (
        P("sp", None),
        P("sp", None),
        P("sp", None),
        P("sp", None),
        P("sp", "tp"),
        P("sp", "tp"),
        P(None, "tp"),
        P("sp", "tp"),
        P(None, "tp"),
        P("sp", None, "tp"),
        P("sp", None, "tp"),
        P("sp", "tp", None),
    )
    out_specs = (
        P("sp", "tp"),
        P("sp", "tp"),
        P("sp", "tp"),
        P("sp", "tp"),
        P("sp", None, "tp"),
        P("sp", None, "tp"),
        P("sp", "tp", None),
    )
    return jax.shard_map(
        on_device, mesh=mesh, in_specs=in_specs, out_specs=out_specs, check_vma=False
    )
```

profile of v0, /device:TPU:27, one launch (start us, length us, event | category | flops | bytes accessed | tf_op | source)
XLA Modules:
  0.0 306.7 jit_solution(16280863391557030212)
XLA Ops:
  7.2 0.0 copy-start
  7.2 0.0 all-gather.4.cloned.1.call-start
  7.2 0.8 broadcast_multiply_fusion
  8.1 0.8 copy.20
  8.9 0.1 eq.29
  9.0 0.1 eq.25
  9.2 0.1 copy.19
  9.3 0.1 mul.430
  9.5 1.1 reduce-window.6
  10.6 0.2 slice_reduce_fusion
  10.9 0.1 fusion.125
  11.0 2.4 scatter_custom_fusion
  13.5 1.0 constant_dynamic-slice_fusion
  14.5 4.0 %gather_fusion = bf16[1024,512]{1,0:T(8,128)(2,1)S(1)} fusion(bf16[257,512]{1,0:T(8,128)(2,1)S(1)} %concatenate.12, s32[1024]{0:T(1024)S(1)} %get-tuple-element.51), kind=kCustom, calls=%fused_computation | custom fusion | bytes 2101248 | tf_op jit(solution)/shard_map/gather | solution.py:55
  18.4 0.0 copy-start.6
  18.5 28.9 %all_to_all.15 = bf16[8,128,512]{2,1,0:T(8,128)(2,1)} all-to-all(bf16[8,128,512]{2,1,0:T(8,128)(2,1)S(1)} %bitcast.117), channel_id=1, replica_groups=mesh['sp'=8,'tp'=4] {'sp'}, dimensions={0} | all-to-all | bytes 2097152 | tf_op jit(solution)/shard_map/all_to_all | solution.py:110
  47.4 0.0 all-gather.4.cloned.1.call-update
  47.4 0.0 all-gather.6.cloned.1.call-start
  47.4 0.1 copy.22
  47.6 0.1 reshape.103
  47.7 1.0 constant_dynamic-slice_fusion.1
  48.7 4.0 %gather_fusion.2 = bf16[1024,512]{1,0:T(8,128)(2,1)S(1)} fusion(bf16[257,512]{1,0:T(8,128)(2,1)S(1)} %concatenate.14, s32[1024]{0:T(1024)S(1)} %get-tuple-element.51), kind=kCustom, calls=%fused_computation.2 | custom fusion | bytes 2101248 | tf_op jit(solution)/shard_map/gather | solution.py:56
  52.7 4.5 %gather_fusion.1 = f32[1024]{0:T(1024)S(1)} fusion(f32[513]{0:T(1024)S(1)} %pad_maximum_fusion.1, s32[1024]{0:T(1024)S(1)} %get-tuple-element.50), kind=kCustom, calls=%fused_computation.1 | custom fusion | bytes 12288 | tf_op jit(solution)/shard_map/gather | solution.py:56
  57.3 0.3 fusion
  57.6 28.8 %all_to_all.16 = bf16[8,128,512]{2,1,0:T(8,128)(2,1)} all-to-all(bf16[8,128,512]{2,1,0:T(8,128)(2,1)S(1)} %fusion), channel_id=1, replica_groups=mesh['sp'=8,'tp'=4] {'sp'}, dimensions={0} | all-to-all | bytes 2097152 | tf_op jit(solution)/shard_map/all_to_all | solution.py:113
  86.4 0.0 all-gather.6.cloned.1.call-update
  86.4 0.2 reduce-scatter.3.cloned.1.call-start
  86.7 0.0 all-gather.4.cloned.1.call-done
  86.7 6.6 %fusion.2 = f32[1024,512]{1,0:T(8,128)} fusion(bf16[1024,2048]{1,0:T(8,128)(2,1)} %bitcast.123, bf16[1,2048,512]{2,1,0:T(8,128)(2,1)} %param.22), kind=kOutput, calls=%fused_computation.12 | convolution fusion | flops 2147483648 | bytes 8388608 | tf_op jit(solution)/shard_map/dot_general | solution.py:64
  93.4 3.6 %fusion.8 = f32[1024,512]{1,0:T(8,128)} fusion(bf16[1024,2048]{1,0:T(8,128)(2,1)S(1)} %bitcast.126, bf16[1,2048,512]{2,1,0:T(8,128)(2,1)S(1)} %copy-done), kind=kOutput, calls=%fused_computation.18 | convolution fusion | flops 2147483648 | bytes 8388608 | tf_op jit(solution)/shard_map/dot_general | solution.py:63
  97.0 25.8 %all-gather.6.cloned.1.call-done = bf16[8,128,2048]{2,1,0:T(8,128)(2,1)} async-done(((bf16[8,128,512]{2,1,0:T(8,128)(2,1)}), bf16[8,128,2048]{2,1,0:T(8,128)(2,1)}) %all-gather.6.cloned.1.call-update) | async-done | bytes 4194320 | tf_op jit(solution)/shard_map/all_gather | solution.py:117
  122.8 7.6 %select_convert_fusion = (bf16[1024,512]{1,0:T(8,128)(2,1)S(1)}, bf16[1024,512]{1,0:T(8,128)(2,1)S(1)}) fusion(f32[1024,512]{1,0:T(8,128)} %fusion.2, f32[1024,512]{1,0:T(8,128)} %fusion.8, bf16[1024,2048]{1,0:T(8,128)(2,1)} %bitcast.127, bf16[1,512,2048]{2,1,0:T(8,128)(2,1)} %param.23), kind=kOutput, calls=%fused_computation.21 | convolution fusion | flops 2159017984 | bytes 12582912 | tf_op jit(solution)/shard_map/dot_general | solution.py:27
  130.5 0.0 copy-start.8
  130.5 2.4 fusion.6
  132.9 4.4 %add_convert_fusion = bf16[1024,2048]{1,0:T(8,128)(2,1)} fusion(f32[1024,2048]{1,0:T(8,128)S(1)} %fusion.6, bf16[1024,512]{1,0:T(8,128)(2,1)S(1)} %get-tuple-element.17, bf16[1,2048,512]{2,1,0:T(8,128)(2,1)S(1)} %copy-done.8), kind=kOutput, calls=%fused_computation.5 | convolution fusion | flops 2151677952 | bytes 15728640 | tf_op jit(solution)/shard_map/dot_general | solution.py:27
  137.3 0.0 reduce-scatter.3.cloned.1.call-update
  137.3 44.0 %reduce-scatter.3.cloned.1.call-done = bf16[1024,512]{1,0:T(8,128)(2,1)} async-done(((bf16[1024,2048]{1,0:T(8,128)(2,1)}), bf16[1024,512]{1,0:T(8,128)(2,1)}) %reduce-scatter.3.cloned.1.call-update) | async-done | bytes 1048592 | tf_op jit(solution)/shard_map/reduce_scatter | solution.py:130
  181.3 5.4 %all-to-all-start.2 = ((bf16[8,128,512]{2,1,0:T(8,128)(2,1)}), bf16[8,128,512]{2,1,0:T(8,128)(2,1)S(1)}, u32[]{:S(2)}, u32[]{:S(2)}) async-start(bf16[8,128,512]{2,1,0:T(8,128)(2,1)} %bitcast.118), calls=%async_computation.3 | async-start | bytes 2097152 | tf_op jit(solution)/shard_map/all_to_all | solution.py:133
  186.8 0.0 all-gather.8.cloned.1.call-start
  186.8 24.1 %all-to-all-done.2 = bf16[8,128,512]{2,1,0:T(8,128)(2,1)S(1)} async-done(((bf16[8,128,512]{2,1,0:T(8,128)(2,1)}), bf16[8,128,512]{2,1,0:T(8,128)(2,1)S(1)}, u32[]{:S(2)}, u32[]{:S(2)}) %all-to-all-start.2) | async-done | bytes 1048608 | tf_op jit(solution)/shard_map/all_to_all | solution.py:133
  210.9 2.6 gather_fusion.3
  213.5 1.7 reshape.108
  215.2 2.1 reduce_sum.58
  217.4 1.9 add_convert_fusion.1
  219.2 0.0 all-gather.8.cloned.1.call-update
  219.3 0.0 reduce-scatter.5.cloned.1.call-start
  219.3 0.1 fusion.103
  219.5 5.5 %all-reduce.3 = (f32[256]{0:T(256)S(1)}, f32[256]{0:T(256)S(1)}) all-reduce(f32[256]{0:T(256)S(1)} %get-tuple-element.10, f32[256]{0:T(256)S(1)} %get-tuple-element.9), channel_id=1, replica_groups=mesh['sp'=8,'tp'=4] {'tp'}, use_global_device_ids=true, to_apply=%region_9.10 | all-reduce | flops 512 | bytes 4096 | tf_op jit(solution)/shard_map/psum | solution.py:146
  225.0 8.5 %convolution_bitcast_fusion = f32[1,512,2048]{2,1,0:T(8,128)} fusion(bf16[1024,2048]{1,0:T(8,128)(2,1)} %bitcast.128, f32[1024,512]{1,0:T(8,128)} %fusion.8, f32[1024,512]{1,0:T(8,128)} %fusion.2), kind=kOutput, calls=%fused_computation.6 | convolution fusion | flops 2152726528 | bytes 12582912 | tf_op jit(solution)/shard_map/dot_general | solution.py:21
  233.5 2.8 all-gather.8.cloned.1.call-done
  236.3 2.8 fusion.119
  239.1 0.0 reduce-scatter.5.cloned.1.call-update
  239.1 0.0 copy-start.9
  239.2 6.7 %convolution_bitcast_fusion.1 = f32[1,2048,512]{2,1,0:T(8,128)} fusion(bf16[1024,2048]{1,0:T(8,128)(2,1)} %bitcast.124, bf16[1024,512]{1,0:T(8,128)(2,1)S(1)} %copy-done.11), kind=kOutput, calls=%fused_computation.7 | convolution fusion | flops 2147483648 | bytes 9437184 | tf_op jit(solution)/shard_map/dot_general | solution.py:21
  245.9 0.5 fusion.138
  246.4 5.3 %all-reduce.2 = (f32[256]{0:T(256)S(1)}, f32[256]{0:T(256)S(1)}) all-reduce(f32[256]{0:T(256)S(1)} %get-tuple-element.8, f32[256]{0:T(256)S(1)} %get-tuple-element.7), channel_id=1, replica_groups=mesh['sp'=8,'tp'=4] {'tp'}, use_global_device_ids=true, to_apply=%region_13.14 | all-reduce | flops 512 | bytes 4096 | tf_op jit(solution)/shard_map/psum | solution.py:157
  251.7 0.2 fusion.116
  252.0 0.0 copy-start.3
  252.0 0.0 copy-start.4
  252.0 2.3 collective-permute-start
  254.3 6.7 %convolution_bitcast_fusion.2 = f32[1,2048,512]{2,1,0:T(8,128)} fusion(bf16[1024,2048]{1,0:T(8,128)(2,1)} %bitcast.125, bf16[1024,512]{1,0:T(8,128)(2,1)S(1)} %copy-done.13), kind=kOutput, calls=%fused_computation.8 | convolution fusion | flops 2147483648 | bytes 9437184 | tf_op jit(solution)/shard_map/dot_general | solution.py:21
  261.0 1.1 multiply_convert_fusion.2
  262.1 0.7 multiply_convert_fusion.3
  262.7 37.5 %reduce-scatter.5.cloned.1.call-done = f32[256,128]{1,0:T(8,128)} async-done(((f32[2048,128]{1,0:T(8,128)}), f32[256,128]{1,0:T(8,128)}) %reduce-scatter.5.cloned.1.call-update) | async-done | bytes 131088 | tf_op jit(solution)/shard_map/reduce_scatter | solution.py:174
  (38 shorter events, 0.2 us)
Async XLA Ops:
  7.2 86.2 %copy-start = (bf16[1,2048,512]{2,1,0:T(8,128)(2,1)S(1)}, bf16[1,2048,512]{2,1,0:T(8,128)(2,1)}, u32[]{:S(2)}) copy-start(bf16[1,2048,512]{2,1,0:T(8,128)(2,1)} %param.21) | copy-start | bytes 6291460
  7.2 79.5 %all-gather.4.cloned.1.call-start = ((), (), s32[]{:S(2)}) async-start(), calls=%async_computation.5 | async-start | bytes 5242880 | tf_op jit(solution)/shard_map/all_gather | solution.py:116
  18.4 29.0 %copy-start.6 = (f32[256,2]{0,1:T(2,128)S(1)}, f32[256,2]{0,1:T(2,128)}, u32[]{:S(2)}) copy-start(f32[256,2]{0,1:T(2,128)} %param.15) | copy-start | bytes 6148
  47.4 75.4 %all-gather.6.cloned.1.call-start = ((), (), s32[]{:S(2)}) async-start(), calls=%async_computation.6 | async-start | bytes 5242880 | tf_op jit(solution)/shard_map/all_gather | solution.py:117
  86.4 94.9 %reduce-scatter.3.cloned.1.call-start = ((), (), s32[]{:S(2)}) async-start(), calls=%async_computation.7 | async-start | bytes 5242880 | tf_op jit(solution)/shard_map/reduce_scatter | solution.py:130
  86.7 6.7 %copy-start.7 = (bf16[8,128,2048]{2,1,0:T(8,128)(2,1)S(1)}, bf16[8,128,2048]{2,1,0:T(8,128)(2,1)}, u32[]{:S(2)}) copy-start(bf16[8,128,2048]{2,1,0:T(8,128)(2,1)} %all-gather.4.cloned.1.call-done) | copy-start | bytes 12582916
  130.5 2.4 copy-start.12
  130.5 2.4 copy-start.10
  130.5 2.4 copy-start.8
  181.3 29.5 %all-to-all-start.2 = ((bf16[8,128,512]{2,1,0:T(8,128)(2,1)}), bf16[8,128,512]{2,1,0:T(8,128)(2,1)S(1)}, u32[]{:S(2)}, u32[]{:S(2)}) async-start(bf16[8,128,512]{2,1,0:T(8,128)(2,1)} %bitcast.118), calls=%async_computation.3 | async-start | bytes 2097152 | tf_op jit(solution)/shard_map/all_to_all | solution.py:133
  186.8 49.6 %all-gather.8.cloned.1.call-start = ((), (), s32[]{:S(2)}) async-start(), calls=%async_computation.8 | async-start | bytes 1310720 | tf_op jit(solution)/shard_map/all_gather | solution.py:144
  213.5 5.8 %copy-start.2 = (bf16[256,128]{1,0:T(8,128)(2,1)S(1)}, bf16[256,128]{1,0:T(8,128)(2,1)}, u32[]{:S(2)}) copy-start(bf16[256,128]{1,0:T(8,128)(2,1)} %param.19) | copy-start | bytes 196612
  213.5 11.5 %copy-start.5 = (f32[31,128]{1,0:T(8,128)S(1)}, f32[31,128]{1,0:T(8,128)}, u32[]{:S(2)}) copy-start(f32[31,128]{1,0:T(8,128)} %param.18) | copy-start | bytes 47620
  219.3 80.9 %reduce-scatter.5.cloned.1.call-start = ((), (), s32[]{:S(2)}) async-start(), calls=%async_computation.9 | async-start | bytes 1179648 | tf_op jit(solution)/shard_map/reduce_scatter | solution.py:174
  233.5 5.6 %copy-start.11 = (bf16[1024,512]{1,0:T(8,128)(2,1)S(1)}, bf16[1024,512]{1,0:T(8,128)(2,1)}, u32[]{:S(2)}) copy-start(bf16[1024,512]{1,0:T(8,128)(2,1)} %copy-done.10) | copy-start | bytes 3145732
  239.1 6.7 %copy-start.1 = (bf16[256,2048]{1,0:T(8,128)(2,1)S(1)}, bf16[256,2048]{1,0:T(8,128)(2,1)}, u32[]{:S(2)}) copy-start(bf16[256,2048]{1,0:T(8,128)(2,1)} %all-gather.8.cloned.1.call-done) | copy-start | bytes 3145732
  239.1 6.7 %copy-start.9 = (bf16[2048,128]{1,0:T(8,128)(2,1)S(1)}, bf16[2048,128]{1,0:T(8,128)(2,1)}, u32[]{:S(2)}) copy-start(bf16[2048,128]{1,0:T(8,128)(2,1)} %param.20) | copy-start | bytes 1572868
  245.9 8.4 %copy-start.13 = (bf16[1024,512]{1,0:T(8,128)(2,1)S(1)}, bf16[1024,512]{1,0:T(8,128)(2,1)}, u32[]{:S(2)}) copy-start(bf16[1024,512]{1,0:T(8,128)(2,1)} %copy-done.12) | copy-start | bytes 3145732
  252.0 9.0 %copy-start.3 = (bf16[256,128]{1,0:T(8,128)(2,1)S(1)}, bf16[256,128]{1,0:T(8,128)(2,1)}, u32[]{:S(2)}) copy-start(bf16[256,128]{1,0:T(8,128)(2,1)} %param.17) | copy-start | bytes 196612
  252.0 9.0 %copy-start.4 = (bf16[256,128]{1,0:T(8,128)(2,1)S(1)}, bf16[256,128]{1,0:T(8,128)(2,1)}, u32[]{:S(2)}) copy-start(bf16[256,128]{1,0:T(8,128)(2,1)} %param.16) | copy-start | bytes 196612
  252.0 9.0 %collective-permute-start = (f32[30,128]{1,0:T(8,128)S(1)}, f32[30,128]{1,0:T(8,128)S(1)}, u32[]{:S(2)}, u32[]{:S(2)}) collective-permute-start(f32[30,128]{1,0:T(8,128)S(1)} %slice.265), channel_id=1, source_target_pairs={{4,0},{8,4},{12,8},{16,12},{20,16},{24,20},{28,24},{5,1},{9,5},{13... | collective-permute-start | bytes 46088 | tf_op jit(solution)/shard_map/ppermute | solution.py:17
Sparse Core Ops, SparseCore 0:
  47.5 36.1 all-gather.3
  86.6 36.2 all-gather.5
  137.4 43.8 reduce-scatter.2
  219.4 16.8 all-gather.7
  240.1 60.0 reduce-scatter.4
where the time goes:
time: 313 us; the launch traced here: 307 us
  waiting for transfers between devices  134 us (43%)
  blocking collectives  68.6 us (22%)
  matrix products  49.9 us (16%)
  local copies, waits for them, and re-layouts  23.2 us (7%)
  between operations  14.1 us (5%)
  other arithmetic  8.58 us (3%)
  starting transfers between devices  8.1 us (3%)
    reduce_scatter x1, waiting for transfers between devices, on_device(): lax.psum_scatter(partial_rows.astype(jnp.bfloat16), 'tp', scatter_dimensi...  44 us
    reduce_scatter x1, waiting for transfers between devices, on_device(): lax.psum_scatter(contract_rows(full_grad, mixed), 'sp', scatter_dimension...  37.5 us
    all_to_all x1, blocking collectives, on_device(): lax.all_to_all(send_rows.reshape(part_shape), 'sp', split_axis=0, concat_...  28.9 us
    all_to_all x1, blocking collectives, on_device(): lax.all_to_all(send_cot.reshape(part_shape), 'sp', split_axis=0, concat_a...  28.8 us
    all_gather x1, waiting for transfers between devices, on_device(): lax.all_gather(part_cot, 'tp', axis=2, tiled=True)  25.8 us
    dot_general x4, matrix products, contract_rows(): lax.dot_general(left, right, (((0,), (0,)), ((), ())), preferred_element_...  24.6 us
    all_to_all x1, waiting for transfers between devices, on_device(): lax.all_to_all(summed_rows.reshape(expert_count, capacity, slice_width),...  24.1 us
    dot_general x3, matrix products, times_transposed(): lax.dot_general(left, right, (((1,), (1,)), ((), ())), preferred_element_...  14.4 us
  transfers between devices with their start and end apart: 7, of which 5 were waited for; matrix products, arithmetic and copies ran while one was open for 15% of the time, Pallas kernels for 0%

commit v1 on v0

--- a/solution.py
+++ b/solution.py
@@ -3,8 +3,6 @@
 from jax import lax
 from jax.sharding import PartitionSpec as P
 
-CW = 512
-
 
 clamp_limit = 7.0
 glu_alpha = 1.702
@@ -29,34 +27,26 @@
     )
 
 
-def block_slots(block_routes, expert_count, capacity):
-    flat_routes = block_routes.reshape(-1)
-    one_hot = (flat_routes[:, None] == jnp.arange(expert_count, dtype=jnp.int32)[None, :]).astype(
-        jnp.int32
-    )
-    earlier = jnp.cumsum(one_hot, axis=0) - one_hot
-    slot_index = jnp.sum(earlier * one_hot, axis=1)
-    target = flat_routes * capacity + slot_index
-    pair_count = flat_routes.shape[0]
-    table = (
-        jnp.full((expert_count * capacity,), pair_count, jnp.int32)
-        .at[target]
-        .set(jnp.arange(pair_count, dtype=jnp.int32))
-    )
-    return (target, table)
-
-
-def gather_pairs(table, block_stream, block_upstream, block_weights, topk):
-    token_of = table // topk
-    zero_row = jnp.zeros((1, block_stream.shape[1]), jnp.bfloat16)
-    stream_pad = jnp.concatenate([block_stream, zero_row], axis=0)
-    upstream_pad = jnp.concatenate([block_upstream, zero_row], axis=0)
-    weight_pad = jnp.concatenate([block_weights.reshape(-1), jnp.zeros((1,), jnp.float32)])
-    send_rows = stream_pad[token_of]
-    send_cot = (weight_pad[table][:, None] * upstream_pad[token_of].astype(jnp.float32)).astype(
-        jnp.bfloat16
-    )
-    return (send_rows, send_cot)
+def pair_rows(block_routes, expert_count, capacity):
+    tok_count, topk = block_routes.shape
+    experts = jnp.arange(expert_count, dtype=jnp.int32)[None, :]
+    hots = [(block_routes[:, k : k + 1] == experts).astype(jnp.float32) for k in range(topk)]
+    before = (
+        jnp.arange(tok_count)[:, None] > jnp.arange(tok_count)[None, :]
+    ).astype(jnp.bfloat16)
+    earlier = jnp.dot(before, sum(hots).astype(jnp.bfloat16), preferred_element_type=jnp.float32)
+    slots = [jnp.sum(earlier * hot, axis=1).astype(jnp.int32) for hot in hots]
+    return [block_routes[:, k] * capacity + slots[k] for k in range(topk)]
+
+
+def select_pairs(targets, block_weights, row_count):
+    rows = jnp.arange(row_count, dtype=jnp.int32)[:, None]
+    hits = [target[None, :] == rows for target in targets]
+    picks = sum(hit.astype(jnp.float32) for hit in hits).astype(jnp.bfloat16)
+    row_weights = jnp.sum(
+        sum(jnp.where(hit, block_weights[:, k][None, :], 0.0) for k, hit in enumerate(hits)), axis=1
+    )
+    return picks, row_weights
 
 
 def expert_backward(expert_rows, expert_cot, gate_weight, up_weight, down_weight):
@@ -96,15 +86,18 @@
 ):
     tok_count = upstream.shape[0]
     model_width = upstream.shape[1]
-    topk = routes.shape[1]
     expert_count = lax.axis_size("sp")
     capacity = 4 * tok_count // expert_count
     slice_width = model_width // lax.axis_size("tp")
     column_start = lax.axis_index("tp") * slice_width
-    target, table = block_slots(routes, expert_count, capacity)
+    targets = pair_rows(routes, expert_count, capacity)
+    picks, row_weights = select_pairs(targets, route_weights, expert_count * capacity)
     stream_part = lax.dynamic_slice_in_dim(stream, column_start, slice_width, 1)
     upstream_part = lax.dynamic_slice_in_dim(upstream, column_start, slice_width, 1)
-    send_rows, send_cot = gather_pairs(table, stream_part, upstream_part, route_weights, topk)
+    send_rows = jnp.dot(picks, stream_part, preferred_element_type=jnp.float32).astype(jnp.bfloat16)
+    send_cot = (
+        row_weights[:, None] * jnp.dot(picks, upstream_part, preferred_element_type=jnp.float32)
+    ).astype(jnp.bfloat16)
     part_shape = (expert_count, capacity, slice_width)
     part_rows, part_cot = (
         lax.all_to_all(
@@ -137,17 +130,17 @@
         concat_axis=0,
         tiled=True,
     )
-    pair_grads = returned.reshape(expert_count * capacity, slice_width)[target].astype(jnp.float32)
-    routed_sum = jnp.sum(pair_grads.reshape(tok_count, topk, slice_width), axis=1)
+    routed_sum = contract_rows(picks, returned.reshape(expert_count * capacity, slice_width))
     upstream_own = lax.dynamic_slice_in_dim(upstream, column_start, slice_width, 1)
     grad_stream = (upstream_own.astype(jnp.float32) + routed_sum).astype(jnp.bfloat16)
     full_grad = lax.all_gather(grad_stream, "tp", axis=1, tiled=True)
+    conv_width = conv_saved.shape[1] * lax.axis_size("tp")
     saved_conv = conv_saved.astype(jnp.float32)
     total_sum, square_sum = lax.psum(
         (jnp.sum(saved_conv, axis=1), jnp.sum(saved_conv * saved_conv, axis=1)), "tp"
     )
-    mean_c = (total_sum / CW)[:, None]
-    var_c = (square_sum / CW)[:, None] - mean_c * mean_c
+    mean_c = (total_sum / conv_width)[:, None]
+    var_c = (square_sum / conv_width)[:, None] - mean_c * mean_c
     inv_std = lax.rsqrt(var_c + norm_eps)
     normed = (saved_conv - mean_c) * inv_std
     norm_sigmoid = jax.nn.sigmoid(normed)
@@ -158,7 +151,7 @@
         (jnp.sum(grad_normed, axis=1), jnp.sum(grad_normed * normed, axis=1)), "tp"
     )
     grad_conv = inv_std * (
-        grad_normed - (first_sum / CW)[:, None] - normed * (second_sum / CW)[:, None]
+        grad_normed - (first_sum / conv_width)[:, None] - normed * (second_sum / conv_width)[:, None]
     )
     kernel_width = conv_taps.shape[0]
     rim_rows = passed_along(grad_conv[: kernel_width - 1], "sp", -1)
@@ -171,9 +164,15 @@
     grad_gate = (grad_glu * glu_value.astype(jnp.float32) * gate_sig * (1.0 - gate_sig)).astype(
         jnp.bfloat16
     )
-    grad_out_proj = lax.psum_scatter(
-        contract_rows(full_grad, mixed), "sp", scatter_dimension=0, tiled=True
-    )
+    proj_parts = contract_rows(full_grad, mixed).astype(jnp.bfloat16)
+    proj_parts = lax.all_to_all(
+        proj_parts.reshape(expert_count, -1, mixed.shape[1]),
+        "sp",
+        split_axis=0,
+        concat_axis=0,
+        tiled=True,
+    )
+    grad_out_proj = jnp.sum(proj_parts.astype(jnp.float32), axis=0)
     return (
         grad_stream,
         grad_value,

time: 313 us -> 258 us (0.82)
  waiting for transfers between devices: 134 us -> 99.5 us
  local copies, waits for them, and re-layouts: 23.2 us -> 0.95 us
  other arithmetic: 8.58 us -> 3.14 us
  starting transfers between devices: 8.1 us -> 13.5 us
    reduce_scatter x1 -> x0, waiting for transfers between devices: 37.5 us -> none  [on_device(): lax.psum_scatter(contract_rows(full_grad, mixed), 'sp', scatter_dimension...]
    gather x4 -> x0, local copies, waits for them, and re-layouts: 15.1 us -> none  [the longest x1 4.53 us: gather_pairs(): weight_pad[table][:, None] * upstream_pad[token_of].astype(jnp.float32)]
    all_to_all x1, waiting for transfers between devices: 24.1 us -> 17.5 us  [on_device(): lax.all_to_all(summed_rows.reshape(expert_count, capacity, slice_width),...]
    all_gather x1, waiting for transfers between devices: 0.02 us -> 5.63 us  [on_device(): lax.all_gather(part_rows, 'tp', axis=2, tiled=True)]
    all_to_all x0 -> x1, starting transfers between devices: none -> 5.44 us  [on_device(): lax.all_to_all(proj_parts.reshape(expert_count, -1, mixed.shape[1]), 'sp'...]
    dot_general x4 -> x5, matrix products: 24.6 us -> 23.4 us  [contract_rows(): lax.dot_general(left, right, (((0,), (0,)), ((), ())), preferred_element_...]
  transfers between devices with their start and end apart: 7 -> 7, of which waited for: 5 -> 6; matrix products, arithmetic and copies ran while one was open for 15% -> 13% of each run, Pallas kernels for 0% -> 0%
where the time goes in v1:
time: 258 us; the launch traced here: 254 us
  waiting for transfers between devices  99.5 us (39%)
  blocking collectives  69.5 us (27%)
  matrix products  53 us (21%)
  between operations  14 us (5%)
  starting transfers between devices  13.5 us (5%)
  other arithmetic  3.14 us (1%)
    reduce_scatter x1, waiting for transfers between devices, on_device(): lax.psum_scatter(partial_rows.astype(jnp.bfloat16), 'tp', scatter_dimensi...  44 us
    all_to_all x1, blocking collectives, on_device(): lax.all_to_all(send_rows.reshape(part_shape), 'sp', split_axis=0, concat_...  28.9 us
    all_to_all x1, blocking collectives, on_device(): lax.all_to_all(send_cot.reshape(part_shape), 'sp', split_axis=0, concat_a...  28.8 us
    all_gather x1, waiting for transfers between devices, on_device(): lax.all_gather(part_cot, 'tp', axis=2, tiled=True)  25.7 us
    dot_general x5, matrix products, contract_rows(): lax.dot_general(left, right, (((0,), (0,)), ((), ())), preferred_element_...  23.4 us
    all_to_all x1, waiting for transfers between devices, on_device(): lax.all_to_all(summed_rows.reshape(expert_count, capacity, slice_width),...  17.5 us
    dot_general x3, matrix products, times_transposed(): lax.dot_general(left, right, (((1,), (1,)), ((), ())), preferred_element_...  14.4 us
    dot_general x1, matrix products, expert_backward(): up_pre = jnp.dot(expert_rows, up_weight, preferred_element_type=jnp.float32)  6.66 us
  transfers between devices with their start and end apart: 7, of which 6 were waited for; matrix products, arithmetic and copies ran while one was open for 13% of the time, Pallas kernels for 0%

profile of v1, /device:TPU:27, one launch (start us, length us, event | category | flops | bytes accessed | tf_op | source)
XLA Modules:
  0.0 253.5 jit_solution(7277678649317412577)
XLA Ops:
  7.2 0.0 copy-start
  7.2 0.0 all-gather.4.cloned.1.call-start
  7.2 0.8 fusion.143
  8.1 0.2 select_reduce_fusion.1
  8.3 0.0 copy-start.5
  8.3 1.4 convolution_convert_fusion.1
  9.7 28.9 %all_to_all.20 = bf16[8,128,512]{2,1,0:T(8,128)(2,1)} all-to-all(bf16[8,128,512]{2,1,0:T(8,128)(2,1)S(1)} %bitcast.111), channel_id=1, replica_groups=mesh['sp'=8,'tp'=4] {'sp'}, dimensions={0} | all-to-all | bytes 2097152 | tf_op jit(solution)/shard_map/all_to_all | solution.py:103
  38.6 0.0 all-gather.4.cloned.1.call-update
  38.7 0.0 all-gather.6.cloned.1.call-start
  38.7 0.0 copy-done.5
  38.7 0.3 add_reduce_fusion
  39.0 1.4 multiply_convert_fusion.1
  40.4 28.8 %all_to_all.21 = bf16[8,128,512]{2,1,0:T(8,128)(2,1)} all-to-all(bf16[8,128,512]{2,1,0:T(8,128)(2,1)S(1)} %bitcast.110), channel_id=1, replica_groups=mesh['sp'=8,'tp'=4] {'sp'}, dimensions={0} | all-to-all | bytes 2097152 | tf_op jit(solution)/shard_map/all_to_all | solution.py:106
  69.3 0.0 all-gather.6.cloned.1.call-update
  69.3 0.0 reduce-scatter.2.cloned.1.call-start
  69.3 5.6 %all-gather.4.cloned.1.call-done = bf16[8,128,2048]{2,1,0:T(8,128)(2,1)} async-done(((bf16[8,128,512]{2,1,0:T(8,128)(2,1)}), bf16[8,128,2048]{2,1,0:T(8,128)(2,1)}) %all-gather.4.cloned.1.call-update) | async-done | bytes 4194320 | tf_op jit(solution)/shard_map/all_gather | solution.py:109
  75.0 6.7 %fusion.1 = f32[1024,512]{1,0:T(8,128)} fusion(bf16[1024,2048]{1,0:T(8,128)(2,1)} %bitcast.118, bf16[1,2048,512]{2,1,0:T(8,128)(2,1)} %param.22), kind=kOutput, calls=%fused_computation.6 | convolution fusion | flops 2147483648 | bytes 8388608 | tf_op jit(solution)/shard_map/dot_general | solution.py:54
  81.6 0.0 copy-done
  81.6 0.0 copy-done.6
  81.6 3.7 %fusion.7 = f32[1024,512]{1,0:T(8,128)} fusion(bf16[1024,2048]{1,0:T(8,128)(2,1)S(1)} %bitcast.121, bf16[1,2048,512]{2,1,0:T(8,128)(2,1)S(1)} %copy-done), kind=kOutput, calls=%fused_computation.12 | convolution fusion | flops 2147483648 | bytes 8388608 | tf_op jit(solution)/shard_map/dot_general | solution.py:53
  85.3 25.7 %all-gather.6.cloned.1.call-done = bf16[8,128,2048]{2,1,0:T(8,128)(2,1)} async-done(((bf16[8,128,512]{2,1,0:T(8,128)(2,1)}), bf16[8,128,2048]{2,1,0:T(8,128)(2,1)}) %all-gather.6.cloned.1.call-update) | async-done | bytes 4194320 | tf_op jit(solution)/shard_map/all_gather | solution.py:110
  111.0 7.6 %select_convert_fusion = (bf16[1024,512]{1,0:T(8,128)(2,1)S(1)}, bf16[1024,512]{1,0:T(8,128)(2,1)S(1)}) fusion(f32[1024,512]{1,0:T(8,128)} %fusion.1, f32[1024,512]{1,0:T(8,128)} %fusion.7, bf16[1024,2048]{1,0:T(8,128)(2,1)} %bitcast.122, bf16[1,512,2048]{2,1,0:T(8,128)(2,1)} %param.23), kind=kOutput, calls=%fused_computation.15 | convolution fusion | flops 2159017984 | bytes 12582912 | tf_op jit(solution)/shard_map/dot_general | solution.py:25
  118.7 0.0 copy-start.11
  118.7 0.0 copy-start.10
  118.7 0.0 copy-start.8
  118.7 2.4 fusion.5
  121.1 0.0 copy-done.11
  121.1 0.0 copy-done.10
  121.1 0.0 copy-done.8
  121.1 4.4 %add_convert_fusion = bf16[1024,2048]{1,0:T(8,128)(2,1)} fusion(f32[1024,2048]{1,0:T(8,128)S(1)} %fusion.5, bf16[1024,512]{1,0:T(8,128)(2,1)S(1)} %get-tuple-element.19, bf16[1,2048,512]{2,1,0:T(8,128)(2,1)S(1)} %copy-done.8), kind=kOutput, calls=%fused_computation | convolution fusion | flops 2151677952 | bytes 15728640 | tf_op jit(solution)/shard_map/dot_general | solution.py:25
  125.5 0.0 reduce-scatter.2.cloned.1.call-update
  125.5 0.0 copy-start.2
  125.5 0.0 copy-start.4
  125.5 44.0 %reduce-scatter.2.cloned.1.call-done = bf16[1024,512]{1,0:T(8,128)(2,1)} async-done(((bf16[1024,2048]{1,0:T(8,128)(2,1)}), bf16[1024,512]{1,0:T(8,128)(2,1)}) %reduce-scatter.2.cloned.1.call-update) | async-done | bytes 1048592 | tf_op jit(solution)/shard_map/reduce_scatter | solution.py:123
  169.5 5.6 %all-to-all-start.2 = ((bf16[8,128,512]{2,1,0:T(8,128)(2,1)}), bf16[8,128,512]{2,1,0:T(8,128)(2,1)S(1)}, u32[]{:S(2)}, u32[]{:S(2)}) async-start(bf16[8,128,512]{2,1,0:T(8,128)(2,1)} %bitcast.108), calls=%async_computation.3 | async-start | bytes 2097152 | tf_op jit(solution)/shard_map/all_to_all | solution.py:126
  175.1 0.0 all-gather.8.cloned.1.call-start
  175.1 0.1 fusion.112
  175.3 6.4 %all-reduce.1 = (f32[256]{0:T(256)S(1)}, f32[256]{0:T(256)S(1)}) all-reduce(f32[256]{0:T(256)S(1)} %get-tuple-element.10, f32[256]{0:T(256)S(1)} %get-tuple-element.9), channel_id=1, replica_groups=mesh['sp'=8,'tp'=4] {'tp'}, use_global_device_ids=true, to_apply=%region_7.8 | all-reduce | flops 512 | bytes 4096 | tf_op jit(solution)/shard_map/psum | solution.py:139
  181.7 17.5 %all-to-all-done.2 = bf16[8,128,512]{2,1,0:T(8,128)(2,1)S(1)} async-done(((bf16[8,128,512]{2,1,0:T(8,128)(2,1)}), bf16[8,128,512]{2,1,0:T(8,128)(2,1)S(1)}, u32[]{:S(2)}, u32[]{:S(2)}) %all-to-all-start.2) | async-done | bytes 1048608 | tf_op jit(solution)/shard_map/all_to_all | solution.py:126
  199.2 2.1 fusion.9
  201.4 0.0 all-gather.8.cloned.1.call-update
  201.4 0.0 copy-start.12
  201.4 7.0 %convolution_bitcast_fusion.1 = f32[1,2048,512]{2,1,0:T(8,128)} fusion(bf16[1024,2048]{1,0:T(8,128)(2,1)} %bitcast.119, bf16[1024,512]{1,0:T(8,128)(2,1)} %copy-done.10), kind=kOutput, calls=%fused_computation.2 | convolution fusion | flops 2147483648 | bytes 9437184 | tf_op jit(solution)/shard_map/dot_general | solution.py:19
  208.5 0.0 copy-done.7
  208.5 0.0 copy-done.13
  208.5 0.0 copy-start.9
  208.5 4.8 %convolution_bitcast_fusion = f32[1,512,2048]{2,1,0:T(8,128)} fusion(bf16[1024,2048]{1,0:T(8,128)(2,1)S(1)} %bitcast.123, f32[1024,512]{1,0:T(8,128)S(1)} %copy-done.13, f32[1024,512]{1,0:T(8,128)S(1)} %copy-done.12), kind=kOutput, calls=%fused_computation.1 | convolution fusion | flops 2152726528 | bytes 12582912 | tf_op jit(solution)/shard_map/dot_general | solution.py:19
  213.3 5.2 %all-gather.8.cloned.1.call-done = bf16[256,2048]{1,0:T(8,128)(2,1)} async-done(((bf16[256,512]{1,0:T(8,128)(2,1)}), bf16[256,2048]{1,0:T(8,128)(2,1)}) %all-gather.8.cloned.1.call-update) | async-done | bytes 1048592 | tf_op jit(solution)/shard_map/all_gather | solution.py:136
  218.5 0.0 copy-done.9
  218.5 1.8 fusion.141
  220.2 5.3 %all-reduce = (f32[256]{0:T(256)S(1)}, f32[256]{0:T(256)S(1)}) all-reduce(f32[256]{0:T(256)S(1)} %get-tuple-element.8, f32[256]{0:T(256)S(1)} %get-tuple-element.7), channel_id=1, replica_groups=mesh['sp'=8,'tp'=4] {'tp'}, use_global_device_ids=true, to_apply=%region_11.12 | all-reduce | flops 512 | bytes 4096 | tf_op jit(solution)/shard_map/psum | solution.py:150
  225.6 2.6 %convolution_convert_fusion = bf16[2048,128]{1,0:T(8,128)(2,1)} fusion(bf16[256,2048]{1,0:T(8,128)(2,1)} %all-gather.8.cloned.1.call-done, bf16[256,128]{1,0:T(8,128)(2,1)S(1)} %copy-done.2, f32[256]{0:T(256)S(1)} %get-tuple-element.57, f32[256]{0:T(256)S(1)} %get-tuple-element.56), kind=kOutput, calls=%fused_computation.4 | convolution fusion | flops 134742016 | bytes 1640448 | tf_op jit(solution)/shard_map/dot_general | solution.py:19
  228.1 5.4 %all-to-all-start.3 = ((bf16[8,256,128]{2,1,0:T(8,128)(2,1)}), bf16[8,256,128]{2,1,0:T(8,128)(2,1)S(1)}, u32[]{:S(2)}, u32[]{:S(2)}) async-start(bf16[8,256,128]{2,1,0:T(8,128)(2,1)} %bitcast.44), calls=%async_computation.4 | async-start | bytes 1048576 | tf_op jit(solution)/shard_map/all_to_all | solution.py:168
  233.6 0.2 fusion.125
  233.8 0.0 copy-start.1
  233.8 0.0 copy-start.3
  233.8 2.3 collective-permute-start
  236.2 6.9 %convolution_bitcast_fusion.2 = f32[1,2048,512]{2,1,0:T(8,128)} fusion(bf16[1024,2048]{1,0:T(8,128)(2,1)} %bitcast.120, bf16[1024,512]{1,0:T(8,128)(2,1)} %copy-done.11), kind=kOutput, calls=%fused_computation.3 | convolution fusion | flops 2147483648 | bytes 9437184 | tf_op jit(solution)/shard_map/dot_general | solution.py:19
  243.0 0.0 collective-permute-done
  243.0 0.0 copy-done.3
  243.0 1.1 multiply_convert_fusion.3
  244.1 0.7 multiply_convert_fusion.4
  244.8 1.5 all-to-all-done.3
  246.2 0.7 convert_reduce_fusion
  (15 shorter events, 0.1 us)
Async XLA Ops:
  7.2 74.5 %copy-start = (bf16[1,2048,512]{2,1,0:T(8,128)(2,1)S(1)}, bf16[1,2048,512]{2,1,0:T(8,128)(2,1)}, u32[]{:S(2)}) copy-start(bf16[1,2048,512]{2,1,0:T(8,128)(2,1)} %param.21) | copy-start | bytes 6291460
  7.2 67.8 %all-gather.4.cloned.1.call-start = ((), (), s32[]{:S(2)}) async-start(), calls=%async_computation.5 | async-start | bytes 5242880 | tf_op jit(solution)/shard_map/all_gather | solution.py:109
  8.3 30.4 %copy-start.5 = (f32[256,2]{0,1:T(2,128)S(1)}, f32[256,2]{0,1:T(2,128)}, u32[]{:S(2)}) copy-start(f32[256,2]{0,1:T(2,128)} %param.15) | copy-start | bytes 6148
  38.7 72.4 %all-gather.6.cloned.1.call-start = ((), (), s32[]{:S(2)}) async-start(), calls=%async_computation.6 | async-start | bytes 5242880 | tf_op jit(solution)/shard_map/all_gather | solution.py:110
  69.3 100.2 %reduce-scatter.2.cloned.1.call-start = ((), (), s32[]{:S(2)}) async-start(), calls=%async_computation.7 | async-start | bytes 5242880 | tf_op jit(solution)/shard_map/reduce_scatter | solution.py:123
  75.0 6.7 %copy-start.6 = (bf16[8,128,2048]{2,1,0:T(8,128)(2,1)S(1)}, bf16[8,128,2048]{2,1,0:T(8,128)(2,1)}, u32[]{:S(2)}) copy-start(bf16[8,128,2048]{2,1,0:T(8,128)(2,1)} %all-gather.4.cloned.1.call-done) | copy-start | bytes 12582916
  118.7 2.4 copy-start.11
  118.7 2.4 copy-start.10
  118.7 2.4 copy-start.8
  125.5 49.6 %copy-start.2 = (bf16[256,128]{1,0:T(8,128)(2,1)S(1)}, bf16[256,128]{1,0:T(8,128)(2,1)}, u32[]{:S(2)}) copy-start(bf16[256,128]{1,0:T(8,128)(2,1)} %param.19) | copy-start | bytes 196612
  125.5 56.2 %copy-start.4 = (f32[31,128]{1,0:T(8,128)S(1)}, f32[31,128]{1,0:T(8,128)}, u32[]{:S(2)}) copy-start(f32[31,128]{1,0:T(8,128)} %param.18) | copy-start | bytes 47620
  169.5 29.7 %all-to-all-start.2 = ((bf16[8,128,512]{2,1,0:T(8,128)(2,1)}), bf16[8,128,512]{2,1,0:T(8,128)(2,1)S(1)}, u32[]{:S(2)}, u32[]{:S(2)}) async-start(bf16[8,128,512]{2,1,0:T(8,128)(2,1)} %bitcast.108), calls=%async_computation.3 | async-start | bytes 2097152 | tf_op jit(solution)/shard_map/all_to_all | solution.py:126
  175.1 43.3 %all-gather.8.cloned.1.call-start = ((), (), s32[]{:S(2)}) async-start(), calls=%async_computation.8 | async-start | bytes 1310720 | tf_op jit(solution)/shard_map/all_gather | solution.py:136
  201.4 7.1 %copy-start.7 = (bf16[8,128,2048]{2,1,0:T(8,128)(2,1)S(1)}, bf16[8,128,2048]{2,1,0:T(8,128)(2,1)}, u32[]{:S(2)}) copy-start(bf16[8,128,2048]{2,1,0:T(8,128)(2,1)} %all-gather.6.cloned.1.call-done) | copy-start | bytes 12582916
  201.4 7.1 %copy-start.12 = (f32[1024,512]{1,0:T(8,128)S(1)}, f32[1024,512]{1,0:T(8,128)}, u32[]{:S(2)}) copy-start(f32[1024,512]{1,0:T(8,128)} %fusion.1) | copy-start | bytes 6291460
  201.4 7.0 %copy-start.13 = (f32[1024,512]{1,0:T(8,128)S(1)}, f32[1024,512]{1,0:T(8,128)}, u32[]{:S(2)}) copy-start(f32[1024,512]{1,0:T(8,128)} %fusion.7) | copy-start | bytes 6291460
  208.5 10.0 %copy-start.9 = (bf16[2048,128]{1,0:T(8,128)(2,1)S(1)}, bf16[2048,128]{1,0:T(8,128)(2,1)}, u32[]{:S(2)}) copy-start(bf16[2048,128]{1,0:T(8,128)(2,1)} %param.20) | copy-start | bytes 1572868
  228.1 18.1 %all-to-all-start.3 = ((bf16[8,256,128]{2,1,0:T(8,128)(2,1)}), bf16[8,256,128]{2,1,0:T(8,128)(2,1)S(1)}, u32[]{:S(2)}, u32[]{:S(2)}) async-start(bf16[8,256,128]{2,1,0:T(8,128)(2,1)} %bitcast.44), calls=%async_computation.4 | async-start | bytes 1048576 | tf_op jit(solution)/shard_map/all_to_all | solution.py:168
  233.8 9.2 %copy-start.1 = (bf16[256,128]{1,0:T(8,128)(2,1)S(1)}, bf16[256,128]{1,0:T(8,128)(2,1)}, u32[]{:S(2)}) copy-start(bf16[256,128]{1,0:T(8,128)(2,1)} %param.17) | copy-start | bytes 196612
  233.8 9.2 %copy-start.3 = (bf16[256,128]{1,0:T(8,128)(2,1)S(1)}, bf16[256,128]{1,0:T(8,128)(2,1)}, u32[]{:S(2)}) copy-start(bf16[256,128]{1,0:T(8,128)(2,1)} %param.16) | copy-start | bytes 196612
  233.8 9.2 %collective-permute-start = (f32[30,128]{1,0:T(8,128)S(1)}, f32[30,128]{1,0:T(8,128)S(1)}, u32[]{:S(2)}, u32[]{:S(2)}) collective-permute-start(f32[30,128]{1,0:T(8,128)S(1)} %slice.266), channel_id=1, source_target_pairs={{4,0},{8,4},{12,8},{16,12},{20,16},{24,20},{28,24},{5,1},{9,5},{13... | collective-permute-start | bytes 46088 | tf_op jit(solution)/shard_map/ppermute | solution.py:15
Sparse Core Ops, SparseCore 0:
  38.8 36.1 all-gather.3
  76.5 34.4 all-gather.5
  125.6 43.8 reduce-scatter.1
  201.5 16.8 all-gather.7

commit v2 on v1

--- a/solution.py
+++ b/solution.py
@@ -1,6 +1,10 @@
+import functools
+
 import jax
 import jax.numpy as jnp
 from jax import lax
+from jax.experimental import pallas as pl
+from jax.experimental.pallas import tpu as pltpu
 from jax.sharding import PartitionSpec as P
 
 
@@ -47,6 +51,284 @@
         sum(jnp.where(hit, block_weights[:, k][None, :], 0.0) for k, hit in enumerate(hits)), axis=1
     )
     return picks, row_weights
+
+
+def greet(sp_count, tp_count):
+    me, lane = lax.axis_index("sp"), lax.axis_index("tp")
+    barrier = pltpu.get_barrier_semaphore()
+    for step in range(1, sp_count):
+        pl.semaphore_signal(
+            barrier,
+            inc=1,
+            device_id={"sp": lax.rem(me + step, sp_count)},
+            device_id_type=pl.DeviceIdType.MESH,
+        )
+    for step in range(1, tp_count):
+        pl.semaphore_signal(
+            barrier,
+            inc=1,
+            device_id={"tp": lax.rem(lane + step, tp_count)},
+            device_id_type=pl.DeviceIdType.MESH,
+        )
+    pl.semaphore_wait(barrier, sp_count + tp_count - 2)
+
+
+def remote(src, dst, send_sem, recv_sem, **target):
+    return pltpu.make_async_remote_copy(
+        src_ref=src,
+        dst_ref=dst,
+        send_sem=send_sem,
+        recv_sem=recv_sem,
+        device_id=target,
+        device_id_type=pl.DeviceIdType.MESH,
+    )
+
+
+def dispatch_kernel(
+    sp_count,
+    tp_count,
+    rows_ref,
+    cot_ref,
+    got_rows,
+    got_cot,
+    far_send,
+    far_recv,
+    side_send,
+    side_recv,
+    pair_send,
+    pair_recv,
+    own_sem,
+):
+    me, lane = lax.axis_index("sp"), lax.axis_index("tp")
+    width = rows_ref.shape[2]
+    chips = tp_count // 2
+    partner = lane + 1 - 2 * lax.rem(lane, 2)
+    sources, results = (rows_ref, cot_ref), (got_rows, got_cot)
+
+    def place(which, block, column):
+        return results[which].at[block, :, pl.ds(pl.multiple_of(column * width, width), width)]
+
+    greet(sp_count, tp_count)
+
+    def far(which, step):
+        to = lax.rem(me + step, sp_count)
+        return remote(
+            sources[which].at[to],
+            place(which, me, lane),
+            far_send.at[which, step],
+            far_recv.at[which, step],
+            sp=to,
+        )
+
+    def beside(which, step, hop):
+        block = lax.rem(me + sp_count - step, sp_count)
+        source = sources[which].at[me] if step == 0 else place(which, block, lane)
+        return remote(
+            source,
+            place(which, block, lane),
+            side_send.at[which, step, hop],
+            side_recv.at[which, step, hop],
+            tp=lax.rem(lane + 2 * hop, tp_count),
+        )
+
+    def paired(which, step, hop):
+        block = lax.rem(me + sp_count - step, sp_count)
+        column = lax.rem(lane + tp_count - 2 * hop, tp_count)
+        source = (
+            sources[which].at[me] if step == 0 and hop == 0 else place(which, block, column)
+        )
+        return remote(
+            source,
+            place(which, block, column),
+            pair_send.at[which, step, hop],
+            pair_recv.at[which, step, hop],
+            tp=partner,
+        )
+
+    started = []
+
+    def begin(copy):
+        copy.start()
+        started.append(copy)
+
+    order = [(which, step) for which in range(2) for step in range(1, sp_count)]
+    own = [
+        pltpu.make_async_copy(sources[which].at[me], place(which, me, lane), own_sem.at[which])
+        for which in range(2)
+    ]
+    for which in range(2):
+        own[which].start()
+        for step in range(1, sp_count):
+            begin(far(which, step))
+    arrivals = []
+    for which in range(2):
+        arrivals += [(which, step) for step in range(sp_count)]
+    lag = 2
+    for at in range(len(arrivals) + lag):
+        if at < len(arrivals):
+            which, step = arrivals[at]
+            if step:
+                far(which, step).wait_recv()
+            for hop in range(1, chips):
+                begin(beside(which, step, hop))
+            begin(paired(which, step, 0))
+        if at >= lag:
+            which, step = arrivals[at - lag]
+            for hop in range(1, chips):
+                beside(which, step, hop).wait_recv()
+                begin(paired(which, step, hop))
+    for which, step in arrivals:
+        for hop in range(chips):
+            paired(which, step, hop).wait_recv()
+    for copy in started:
+        copy.wait_send()
+    for copy in own:
+        copy.wait()
+
+
+def dispatch(send_rows, send_cot, sp_count, tp_count):
+    blocks, capacity, width = send_rows.shape
+    full = jax.ShapeDtypeStruct((blocks, capacity, width * tp_count), send_rows.dtype)
+    dma = pltpu.SemaphoreType.DMA
+    chips = tp_count // 2
+    return pl.pallas_call(
+        functools.partial(dispatch_kernel, sp_count, tp_count),
+        out_shape=(full, full),
+        in_specs=[pl.BlockSpec(memory_space=pltpu.VMEM)] * 2,
+        out_specs=[pl.BlockSpec(memory_space=pl.ANY)] * 2,
+        scratch_shapes=[dma((2, sp_count))] * 2
+        + [dma((2, sp_count, chips))] * 4
+        + [dma((2,))],
+        compiler_params=pltpu.CompilerParams(collective_id=0, has_side_effects=True),
+        name="dispatch",
+    )(send_rows, send_cot)
+
+
+def return_kernel(
+    sp_count,
+    tp_count,
+    partial_ref,
+    out_ref,
+    pair_in,
+    side_out,
+    side_in,
+    total,
+    pair_send,
+    pair_recv,
+    side_send,
+    side_recv,
+    far_send,
+    far_recv,
+):
+    me, lane = lax.axis_index("sp"), lax.axis_index("tp")
+    width = out_ref.shape[2]
+    chips = tp_count // 2
+    core = lax.rem(lane, 2)
+    partner = lane + 1 - 2 * core
+
+    greet(sp_count, tp_count)
+    started = []
+
+    def begin(copy):
+        copy.start()
+        started.append(copy)
+
+    def columns(column):
+        return pl.ds(pl.multiple_of(column * width, width), width)
+
+    def swapped(step, hop):
+        block = lax.rem(me + step, sp_count)
+        chip_lane = lax.rem(lane + 2 * hop, tp_count)
+        other = chip_lane + 1 - 2 * core
+        return remote(
+            partial_ref.at[block, :, columns(other)],
+            pair_in.at[step, hop],
+            pair_send.at[step, hop],
+            pair_recv.at[step, hop],
+            tp=partner,
+        )
+
+    def beside(step, hop):
+        return remote(
+            side_out.at[step, hop - 1],
+            side_in.at[step, hop - 1],
+            side_send.at[step, hop - 1],
+            side_recv.at[step, hop - 1],
+            tp=lax.rem(lane + 2 * hop, tp_count),
+        )
+
+    def far(step):
+        return remote(
+            total.at[step],
+            out_ref.at[me],
+            far_send.at[step],
+            far_recv.at[step],
+            sp=lax.rem(me + step, sp_count),
+        )
+
+    order = list(range(1, sp_count)) + [0]
+    for step in order:
+        for hop in list(range(1, chips)) + [0]:
+            begin(swapped(step, hop))
+
+    def pair_sum(step, hop):
+        block = lax.rem(me + step, sp_count)
+        column = lax.rem(lane + 2 * hop, tp_count)
+        return partial_ref[block, :, columns(column)].astype(jnp.float32) + pair_in[
+            step, hop
+        ].astype(jnp.float32)
+
+    lag = 2
+    for at in range(sp_count + lag):
+        if at < sp_count:
+            step = order[at]
+            for hop in range(1, chips):
+                swapped(step, hop).wait_recv()
+                side_out[step, hop - 1] = pair_sum(step, hop).astype(jnp.bfloat16)
+                begin(beside(step, hop))
+        if at >= lag:
+            step = order[at - lag]
+            swapped(step, 0).wait_recv()
+            value = pair_sum(step, 0)
+            for hop in range(1, chips):
+                beside(step, hop).wait_recv()
+                value += side_in[step, hop - 1].astype(jnp.float32)
+            if step:
+                total[step] = value.astype(jnp.bfloat16)
+                begin(far(step))
+            else:
+                out_ref[me] = value.astype(jnp.bfloat16)
+    for step in range(1, sp_count):
+        far(step).wait_recv()
+    for copy in started:
+        copy.wait_send()
+
+
+def send_back(partial_rows, sp_count, tp_count):
+    blocks, capacity, model_width = partial_rows.shape
+    width = model_width // tp_count
+    chips = tp_count // 2
+    dma, vmem = pltpu.SemaphoreType.DMA, pltpu.VMEM
+    return pl.pallas_call(
+        functools.partial(return_kernel, sp_count, tp_count),
+        out_shape=jax.ShapeDtypeStruct((blocks, capacity, width), jnp.bfloat16),
+        in_specs=[pl.BlockSpec(memory_space=vmem)],
+        out_specs=pl.BlockSpec(memory_space=vmem),
+        scratch_shapes=[
+            vmem((sp_count, chips, capacity, width), jnp.bfloat16),
+            vmem((sp_count, chips - 1, capacity, width), jnp.bfloat16),
+            vmem((sp_count, chips - 1, capacity, width), jnp.bfloat16),
+            vmem((sp_count, capacity, width), jnp.bfloat16),
+            dma((sp_count, chips)),
+            dma((sp_count, chips)),
+            dma((sp_count, chips - 1)),
+            dma((sp_count, chips - 1)),
+            dma((sp_count,)),
+            dma((sp_count,)),
+        ],
+        compiler_params=pltpu.CompilerParams(collective_id=1, has_side_effects=True),
+        name="send_back",
+    )(partial_rows)
 
 
 def expert_backward(expert_rows, expert_cot, gate_weight, up_weight, down_weight):
@@ -99,15 +381,11 @@
         row_weights[:, None] * jnp.dot(picks, upstream_part, preferred_element_type=jnp.float32)
     ).astype(jnp.bfloat16)
     part_shape = (expert_count, capacity, slice_width)
-    part_rows, part_cot = (
-        lax.all_to_all(
-            send_rows.reshape(part_shape), "sp", split_axis=0, concat_axis=0, tiled=True
-        ),
-        lax.all_to_all(send_cot.reshape(part_shape), "sp", split_axis=0, concat_axis=0, tiled=True),
-    )
-    got_rows, got_cot = (
-        lax.all_gather(part_rows, "tp", axis=2, tiled=True),
-        lax.all_gather(part_cot, "tp", axis=2, tiled=True),
+    got_rows, got_cot = dispatch(
+        send_rows.reshape(part_shape),
+        send_cot.reshape(part_shape),
+        expert_count,
+        lax.axis_size("tp"),
     )
     expert_rows = got_rows.reshape(-1, model_width)
     expert_cot = got_cot.reshape(-1, model_width)
@@ -120,15 +398,10 @@
     partial_rows = times_transposed(grad_gate_pre, gate_weight) + times_transposed(
         grad_up_pre, up_weight
     )
-    summed_rows = lax.psum_scatter(
-        partial_rows.astype(jnp.bfloat16), "tp", scatter_dimension=1, tiled=True
-    )
-    returned = lax.all_to_all(
-        summed_rows.reshape(expert_count, capacity, slice_width),
-        "sp",
-        split_axis=0,
-        concat_axis=0,
-        tiled=True,
+    returned = send_back(
+        partial_rows.astype(jnp.bfloat16).reshape(expert_count, capacity, model_width),
+        expert_count,
+        lax.axis_size("tp"),
     )
     routed_sum = contract_rows(picks, returned.reshape(expert_count * capacity, slice_width))
     upstream_own = lax.dynamic_slice_in_dim(upstream, column_start, slice_width, 1)

time: 258 us -> 206 us (0.80)
  the two profiles are of different devices: /device:TPU:27 before, /device:TPU:0 now
where the time goes in v2:
time: 206 us
  Pallas kernels  111 us (54%)
  matrix products  48.8 us (24%)
  between operations  14.3 us (7%)
  blocking collectives  12.2 us (6%)
  starting transfers between devices  8.13 us (4%)
  waiting for transfers between devices  4.34 us (2%)
  local copies, waits for them, and re-layouts  3.61 us (2%)
  other arithmetic  3.09 us (2%)
    pallas_call x1, Pallas kernels, dispatch(): pl.pallas_call(functools.partial(dispatch_kernel, sp_count, tp_count), ou...  64.3 us
    pallas_call x1, Pallas kernels, send_back(): pl.pallas_call(functools.partial(return_kernel, sp_count, tp_count), out_...  47 us
    dot_general x5, matrix products, contract_rows(): lax.dot_general(left, right, (((0,), (0,)), ((), ())), preferred_element_...  23.8 us
    dot_general x3, matrix products, times_transposed(): lax.dot_general(left, right, (((1,), (1,)), ((), ())), preferred_element_...  10.5 us
    all_to_all x1, starting transfers between devices, on_device(): lax.all_to_all(proj_parts.reshape(expert_count, -1, mixed.shape[1]), 'sp'...  6.8 us
    psum x1, blocking collectives, on_device(): lax.psum((jnp.sum(saved_conv, axis=1), jnp.sum(saved_conv * saved_conv, a...  6.28 us
    psum x1, blocking collectives, on_device(): lax.psum((jnp.sum(grad_normed, axis=1), jnp.sum(grad_normed * normed, axi...  5.96 us
    dot_general x1, matrix products, expert_backward(): up_pre = jnp.dot(expert_rows, up_weight, preferred_element_type=jnp.float32)  5.33 us
  transfers between devices with their start and end apart: 3, of which 1 were waited for; matrix products, arithmetic and copies ran while one was open for 11% of the time, Pallas kernels for 0%

profile of v2, /device:TPU:0, one launch (start us, length us, event | category | flops | bytes accessed | tf_op | source)
XLA Modules:
  0.0 205.8 jit_solution(15835068844175142450)
XLA Ops:
  7.2 0.0 copy-start
  7.2 0.0 all-gather.2.cloned.1.call-start
  7.2 0.8 fusion.144
  8.1 0.8 fusion.143
  8.8 0.2 select_reduce_fusion.1
  9.1 0.3 add_reduce_fusion
  9.3 2.4 %convolution_convert_fusion.1 = bf16[1024,512]{1,0:T(8,128)(2,1)} fusion(s32[256]{0:T(256)S(1)} %get-tuple-element.63, s32[256]{0:T(256)S(1)} %get-tuple-element.64, bf16[256,2048]{1,0:T(8,128)(2,1)} %param.13, s32[]{:T(128)S(6)} %select_n.19), kind=kOutput, calls=%fused_computation.50 | convolution fusion | flops 270532608 | bytes 1312772 | tf_op jit(solution)/shard_map/dot_general | solution.py:379
  11.7 2.4 %multiply_convert_fusion.1 = bf16[1024,512]{1,0:T(8,128)(2,1)} fusion(f32[1024]{0:T(1024)S(1)} %add_reduce_fusion, s32[256]{0:T(256)S(1)} %get-tuple-element.63, s32[256]{0:T(256)S(1)} %get-tuple-element.64, bf16[256,2048]{1,0:T(8,128)(2,1)} %param.12, s32[]{:T(128)S(6)} %select_n.19), kind=kOutput, calls=%fused_computation.20 | convolution fusion | flops 271056896 | bytes 1316868 | tf_op jit(solution)/shard_map/dot_general | solution.py:381
  14.1 64.3 %dispatch.1 = (bf16[8,128,2048]{2,1,0:T(8,128)(2,1)}, bf16[8,128,2048]{2,1,0:T(8,128)(2,1)}) custom-call(bf16[8,128,512]{2,1,0:T(8,128)(2,1)} %bitcast.110, bf16[8,128,512]{2,1,0:T(8,128)(2,1)} %bitcast.111), custom_call_target="tpu_custom_call" | custom-call | tf_op jit(solution)/shard_map/dispatch/pallas_call | solution.py:194
  78.4 0.0 copy-start.7
  78.4 5.3 %fusion.1 = f32[1024,512]{1,0:T(8,128)S(1)} fusion(bf16[1024,2048]{1,0:T(8,128)(2,1)} %bitcast.120, bf16[1,2048,512]{2,1,0:T(8,128)(2,1)} %param.22), kind=kOutput, calls=%fused_computation.6 | convolution fusion | flops 2147483648 | bytes 8388608 | tf_op jit(solution)/shard_map/dot_general | solution.py:336
  83.7 0.0 copy-done
  83.8 0.0 copy-done.7
  83.8 0.0 copy-start.12
  83.8 0.0 copy-start.5
  83.8 0.0 copy-start.8
  83.8 2.3 %fusion.7 = f32[1024,512]{1,0:T(8,128)S(1)} fusion(bf16[1024,2048]{1,0:T(8,128)(2,1)S(1)} %bitcast.123, bf16[1,2048,512]{2,1,0:T(8,128)(2,1)S(1)} %copy-done), kind=kOutput, calls=%fused_computation.12 | convolution fusion | flops 2147483648 | bytes 8388608 | tf_op jit(solution)/shard_map/dot_general | solution.py:335
  86.1 0.0 copy-start.14
  86.1 0.0 copy-done.12
  86.1 0.6 copy-done.5
  86.7 1.3 copy-done.8
  88.0 3.6 %select_convert_fusion = (bf16[1024,512]{1,0:T(8,128)(2,1)S(1)}, bf16[1024,512]{1,0:T(8,128)(2,1)S(1)}) fusion(f32[1024,512]{1,0:T(8,128)S(1)} %fusion.1, f32[1024,512]{1,0:T(8,128)S(1)} %fusion.7, bf16[1024,2048]{1,0:T(8,128)(2,1)S(1)} %bitcast.118, bf16[1,512,2048]{2,1,0:T(8,128)(2,1)S(1)} %copy-done.8), kind=kOutput, calls=%fused_computation.15 | convolution fusion | flops 2159017984 | bytes 12582912 | tf_op jit(solution)/shard_map/dot_general | solution.py:29
  91.6 0.0 copy-done.14
  91.7 0.0 copy-start.11
  91.7 0.0 copy-start.10
  91.7 0.0 copy-start.9
  91.7 2.4 %fusion.5 = f32[1024,2048]{1,0:T(8,128)S(1)} fusion(bf16[1024,512]{1,0:T(8,128)(2,1)S(1)} %get-tuple-element.24, bf16[1,2048,512]{2,1,0:T(8,128)(2,1)S(1)} %copy-done), kind=kOutput, calls=%fused_computation.10 | convolution fusion | flops 2147483648 | bytes 11534336 | tf_op jit(solution)/shard_map/dot_general | solution.py:29
  94.1 0.0 copy-done.11
  94.1 0.0 copy-done.10
  94.1 0.0 copy-done.9
  94.1 4.6 %add_convert_fusion = bf16[1024,2048]{1,0:T(8,128)(2,1)} fusion(f32[1024,2048]{1,0:T(8,128)S(1)} %fusion.5, bf16[1024,512]{1,0:T(8,128)(2,1)S(1)} %get-tuple-element.23, bf16[1,2048,512]{2,1,0:T(8,128)(2,1)S(1)} %copy-done.9), kind=kOutput, calls=%fused_computation | convolution fusion | flops 2151677952 | bytes 15728640 | tf_op jit(solution)/shard_map/dot_general | solution.py:29
  98.7 47.0 %send_back.1 = bf16[8,128,512]{2,1,0:T(8,128)(2,1)} custom-call(bf16[8,128,2048]{2,1,0:T(8,128)(2,1)} %bitcast.108), custom_call_target="tpu_custom_call" | custom-call | tf_op jit(solution)/shard_map/send_back/pallas_call | solution.py:312
  145.7 2.5 %fusion.9 = bf16[256,512]{1,0:T(8,128)(2,1)} fusion(bf16[1024,512]{1,0:T(8,128)(2,1)} %bitcast.109, s32[256]{0:T(256)S(1)} %get-tuple-element.63, s32[256]{0:T(256)S(1)} %get-tuple-element.64, bf16[256,2048]{1,0:T(8,128)(2,1)} %param.12, s32[]{:T(128)S(6)} %select_n.19), kind=kOutput, calls=%fused_computation.52 | convolution fusion | flops 270401536 | bytes 1574916 | tf_op jit(solution)/shard_map/dot_general | solution.py:23
  148.1 0.0 all-gather.2.cloned.1.call-update
  148.2 0.0 copy-start.2
  148.2 0.0 copy-start.4
  148.2 6.9 %convolution_bitcast_fusion.1 = f32[1,2048,512]{2,1,0:T(8,128)} fusion(bf16[1024,2048]{1,0:T(8,128)(2,1)} %bitcast.121, bf16[1024,512]{1,0:T(8,128)(2,1)} %copy-done.10), kind=kOutput, calls=%fused_computation.2 | convolution fusion | flops 2147483648 | bytes 9437184 | tf_op jit(solution)/shard_map/dot_general | solution.py:23
  155.1 0.0 copy-done.2
  155.1 0.1 fusion.112
  155.2 0.0 copy-done.4
  155.3 6.3 %all-reduce.1 = (f32[256]{0:T(256)S(1)}, f32[256]{0:T(256)S(1)}) all-reduce(f32[256]{0:T(256)S(1)} %get-tuple-element.14, f32[256]{0:T(256)S(1)} %get-tuple-element.13), channel_id=1, replica_groups=mesh['sp'=8,'tp'=4] {'tp'}, use_global_device_ids=true, to_apply=%region_6.7 | all-reduce | flops 512 | bytes 4096 | tf_op jit(solution)/shard_map/psum | solution.py:412
  161.6 0.0 copy-start.6
  161.6 0.0 copy-start.13
  161.6 0.0 copy-start.15
  161.6 7.1 %convolution_bitcast_fusion.2 = f32[1,2048,512]{2,1,0:T(8,128)} fusion(bf16[1024,2048]{1,0:T(8,128)(2,1)} %bitcast.122, bf16[1024,512]{1,0:T(8,128)(2,1)} %copy-done.11), kind=kOutput, calls=%fused_computation.3 | convolution fusion | flops 2147483648 | bytes 9437184 | tf_op jit(solution)/shard_map/dot_general | solution.py:23
  168.6 0.0 copy-done.6
  168.6 0.0 copy-done.13
  168.6 0.0 copy-done.15
  168.6 4.8 %convolution_bitcast_fusion = f32[1,512,2048]{2,1,0:T(8,128)} fusion(bf16[1024,2048]{1,0:T(8,128)(2,1)S(1)} %bitcast.119, f32[1024,512]{1,0:T(8,128)S(1)} %copy-done.15, f32[1024,512]{1,0:T(8,128)S(1)} %copy-done.13), kind=kOutput, calls=%fused_computation.1 | convolution fusion | flops 2152726528 | bytes 12582912 | tf_op jit(solution)/shard_map/dot_general | solution.py:23
  173.4 0.0 all-gather.2.cloned.1.call-done
  173.4 2.6 %convolution_convert_fusion = bf16[2048,128]{1,0:T(8,128)(2,1)} fusion(bf16[256,2048]{1,0:T(8,128)(2,1)} %all-gather.2.cloned.1.call-done, bf16[256,128]{1,0:T(8,128)(2,1)S(1)} %copy-done.2, f32[256]{0:T(256)S(1)} %get-tuple-element.61, f32[256]{0:T(256)S(1)} %get-tuple-element.60), kind=kOutput, calls=%fused_computation.4 | convolution fusion | flops 134742016 | bytes 1640448 | tf_op jit(solution)/shard_map/dot_general | solution.py:23
  176.0 0.0 copy-start.1
  176.0 6.8 %all-to-all-start = ((bf16[8,256,128]{2,1,0:T(8,128)(2,1)}), bf16[8,256,128]{2,1,0:T(8,128)(2,1)S(1)}, u32[]{:S(2)}, u32[]{:S(2)}) async-start(bf16[8,256,128]{2,1,0:T(8,128)(2,1)} %bitcast.44), calls=%async_computation | async-start | bytes 1048576 | tf_op jit(solution)/shard_map/all_to_all | solution.py:441
  182.8 1.9 fusion.141
  184.7 6.0 %all-reduce = (f32[256]{0:T(256)S(1)}, f32[256]{0:T(256)S(1)}) all-reduce(f32[256]{0:T(256)S(1)} %get-tuple-element.12, f32[256]{0:T(256)S(1)} %get-tuple-element.11), channel_id=1, replica_groups=mesh['sp'=8,'tp'=4] {'tp'}, use_global_device_ids=true, to_apply=%region_10.11 | all-reduce | flops 512 | bytes 4096 | tf_op jit(solution)/shard_map/psum | solution.py:423
  190.7 0.2 fusion.125
  190.9 1.3 collective-permute-start
  192.2 4.3 %collective-permute-done = f32[30,128]{1,0:T(8,128)S(1)} collective-permute-done((f32[30,128]{1,0:T(8,128)S(1)}, f32[30,128]{1,0:T(8,128)S(1)}, u32[]{:S(2)}, u32[]{:S(2)}) %collective-permute-start) | collective-permute-done | bytes 15392 | tf_op jit(solution)/shard_map/ppermute | solution.py:19
  196.6 0.0 copy-done.1
  196.6 0.0 copy-done.3
  196.6 1.0 multiply_convert_fusion.3
  197.6 0.7 multiply_convert_fusion.4
  198.3 0.0 all-to-all-done
  198.3 0.7 convert_reduce_fusion
  (8 shorter events, 0.1 us)
Async XLA Ops:
  7.2 76.6 %copy-start = (bf16[1,2048,512]{2,1,0:T(8,128)(2,1)S(1)}, bf16[1,2048,512]{2,1,0:T(8,128)(2,1)}, u32[]{:S(2)}) copy-start(bf16[1,2048,512]{2,1,0:T(8,128)(2,1)} %param.21) | copy-start | bytes 6291460
  7.2 166.3 %all-gather.2.cloned.1.call-start = ((), (), s32[]{:S(2)}) async-start(), calls=%async_computation.1 | async-start | bytes 1310720 | tf_op jit(solution)/shard_map/all_gather | solution.py:409
  78.4 5.4 %copy-start.7 = (bf16[8,128,2048]{2,1,0:T(8,128)(2,1)S(1)}, bf16[8,128,2048]{2,1,0:T(8,128)(2,1)}, u32[]{:S(2)}) copy-start(bf16[8,128,2048]{2,1,0:T(8,128)(2,1)} %get-tuple-element.9) | copy-start | bytes 12582916
  83.8 2.4 %copy-start.12 = (f32[1024,512]{1,0:T(8,128)}, f32[1024,512]{1,0:T(8,128)S(1)}, u32[]{:S(2)}) copy-start(f32[1024,512]{1,0:T(8,128)S(1)} %fusion.1) | copy-start | bytes 6291460
  83.8 2.9 %copy-start.5 = (bf16[8,128,2048]{2,1,0:T(8,128)(2,1)S(1)}, bf16[8,128,2048]{2,1,0:T(8,128)(2,1)}, u32[]{:S(2)}) copy-start(bf16[8,128,2048]{2,1,0:T(8,128)(2,1)} %get-tuple-element.10) | copy-start | bytes 12582916
  83.8 4.3 %copy-start.8 = (bf16[1,512,2048]{2,1,0:T(8,128)(2,1)S(1)}, bf16[1,512,2048]{2,1,0:T(8,128)(2,1)}, u32[]{:S(2)}) copy-start(bf16[1,512,2048]{2,1,0:T(8,128)(2,1)} %param.23) | copy-start | bytes 6291460
  86.1 5.5 %copy-start.14 = (f32[1024,512]{1,0:T(8,128)}, f32[1024,512]{1,0:T(8,128)S(1)}, u32[]{:S(2)}) copy-start(f32[1024,512]{1,0:T(8,128)S(1)} %fusion.7) | copy-start | bytes 6291460
  91.7 2.4 %copy-start.11 = (bf16[1024,512]{1,0:T(8,128)(2,1)}, bf16[1024,512]{1,0:T(8,128)(2,1)S(1)}, u32[]{:S(2)}) copy-start(bf16[1024,512]{1,0:T(8,128)(2,1)S(1)} %get-tuple-element.24) | copy-start | bytes 3145732
  91.7 2.4 %copy-start.10 = (bf16[1024,512]{1,0:T(8,128)(2,1)}, bf16[1024,512]{1,0:T(8,128)(2,1)S(1)}, u32[]{:S(2)}) copy-start(bf16[1024,512]{1,0:T(8,128)(2,1)S(1)} %get-tuple-element.23) | copy-start | bytes 3145732
  91.7 2.4 %copy-start.9 = (bf16[1,2048,512]{2,1,0:T(8,128)(2,1)S(1)}, bf16[1,2048,512]{2,1,0:T(8,128)(2,1)}, u32[]{:S(2)}) copy-start(bf16[1,2048,512]{2,1,0:T(8,128)(2,1)} %param.22) | copy-start | bytes 6291460
  148.2 6.9 %copy-start.2 = (bf16[256,128]{1,0:T(8,128)(2,1)S(1)}, bf16[256,128]{1,0:T(8,128)(2,1)}, u32[]{:S(2)}) copy-start(bf16[256,128]{1,0:T(8,128)(2,1)} %param.19) | copy-start | bytes 196612
  148.2 7.1 %copy-start.4 = (f32[31,128]{1,0:T(8,128)S(1)}, f32[31,128]{1,0:T(8,128)}, u32[]{:S(2)}) copy-start(f32[31,128]{1,0:T(8,128)} %param.18) | copy-start | bytes 47620
  161.6 7.1 %copy-start.6 = (bf16[8,128,2048]{2,1,0:T(8,128)(2,1)S(1)}, bf16[8,128,2048]{2,1,0:T(8,128)(2,1)}, u32[]{:S(2)}) copy-start(bf16[8,128,2048]{2,1,0:T(8,128)(2,1)} %get-tuple-element.10) | copy-start | bytes 12582916
  161.6 7.1 %copy-start.13 = (f32[1024,512]{1,0:T(8,128)S(1)}, f32[1024,512]{1,0:T(8,128)}, u32[]{:S(2)}) copy-start(f32[1024,512]{1,0:T(8,128)} %copy-done.12) | copy-start | bytes 6291460
  161.6 7.1 %copy-start.15 = (f32[1024,512]{1,0:T(8,128)S(1)}, f32[1024,512]{1,0:T(8,128)}, u32[]{:S(2)}) copy-start(f32[1024,512]{1,0:T(8,128)} %copy-done.14) | copy-start | bytes 6291460
  176.0 20.5 %copy-start.1 = (bf16[256,128]{1,0:T(8,128)(2,1)S(1)}, bf16[256,128]{1,0:T(8,128)(2,1)}, u32[]{:S(2)}) copy-start(bf16[256,128]{1,0:T(8,128)(2,1)} %param.17) | copy-start | bytes 196612
  176.0 20.5 %copy-start.3 = (bf16[256,128]{1,0:T(8,128)(2,1)S(1)}, bf16[256,128]{1,0:T(8,128)(2,1)}, u32[]{:S(2)}) copy-start(bf16[256,128]{1,0:T(8,128)(2,1)} %param.16) | copy-start | bytes 196612
  176.0 22.2 %all-to-all-start = ((bf16[8,256,128]{2,1,0:T(8,128)(2,1)}), bf16[8,256,128]{2,1,0:T(8,128)(2,1)S(1)}, u32[]{:S(2)}, u32[]{:S(2)}) async-start(bf16[8,256,128]{2,1,0:T(8,128)(2,1)} %bitcast.44), calls=%async_computation | async-start | bytes 1048576 | tf_op jit(solution)/shard_map/all_to_all | solution.py:441
  190.9 5.6 %collective-permute-start = (f32[30,128]{1,0:T(8,128)S(1)}, f32[30,128]{1,0:T(8,128)S(1)}, u32[]{:S(2)}, u32[]{:S(2)}) collective-permute-start(f32[30,128]{1,0:T(8,128)S(1)} %slice.266), channel_id=1, source_target_pairs={{4,0},{8,4},{12,8},{16,12},{20,16},{24,20},{28,24},{5,1},{9,5},{13... | collective-permute-start | bytes 46088 | tf_op jit(solution)/shard_map/ppermute | solution.py:19
Sparse Core Ops, SparseCore 0:
  148.3 18.0 all-gather.1

commit v3 on v2

--- a/solution.py
+++ b/solution.py
@@ -11,12 +11,6 @@
 clamp_limit = 7.0
 glu_alpha = 1.702
 norm_eps = 1e-05
-
-
-def passed_along(shard, axis, by):
-    size = lax.axis_size(axis)
-    pairs = [(i, i + by) for i in range(size) if 0 <= i + by < size]
-    return lax.ppermute(shard, axis, pairs)
 
 
 def contract_rows(left, right):
@@ -204,27 +198,57 @@
     )(send_rows, send_cot)
 
 
-def return_kernel(
+def tail_kernel(
     sp_count,
     tp_count,
     partial_ref,
-    out_ref,
+    picks_ref,
+    upstream_ref,
+    saved_ref,
+    proj_ref,
+    taps_ref,
+    value_ref,
+    gate_ref,
+    grad_stream_ref,
+    grad_value_ref,
+    grad_gate_ref,
+    grad_proj_ref,
     pair_in,
     side_out,
     side_in,
     total,
+    returned,
+    full,
+    stat_out,
+    stat_in,
+    parts_out,
+    parts_in,
+    rim_in,
+    padded,
     pair_send,
     pair_recv,
     side_send,
     side_recv,
     far_send,
     far_recv,
+    full_send,
+    full_recv,
+    stat_send,
+    stat_recv,
+    parts_send,
+    parts_recv,
+    rim_send,
+    rim_recv,
 ):
     me, lane = lax.axis_index("sp"), lax.axis_index("tp")
-    width = out_ref.shape[2]
+    width = returned.shape[2]
     chips = tp_count // 2
     core = lax.rem(lane, 2)
     partner = lane + 1 - 2 * core
+    tok_count, channels = saved_ref.shape
+    conv_width = channels * tp_count
+    groups = tok_count // 128
+    f32, bf16 = jnp.float32, jnp.bfloat16
 
     greet(sp_count, tp_count)
     started = []
@@ -238,8 +262,7 @@
 
     def swapped(step, hop):
         block = lax.rem(me + step, sp_count)
-        chip_lane = lax.rem(lane + 2 * hop, tp_count)
-        other = chip_lane + 1 - 2 * core
+        other = lax.rem(lane + 2 * hop, tp_count) + 1 - 2 * core
         return remote(
             partial_ref.at[block, :, columns(other)],
             pair_in.at[step, hop],
@@ -260,7 +283,7 @@
     def far(step):
         return remote(
             total.at[step],
-            out_ref.at[me],
+            returned.at[me],
             far_send.at[step],
             far_recv.at[step],
             sp=lax.rem(me + step, sp_count),
@@ -271,12 +294,60 @@
         for hop in list(range(1, chips)) + [0]:
             begin(swapped(step, hop))
 
+    eye = (
+        lax.broadcasted_iota(jnp.int32, (128, 128), 0)
+        == lax.broadcasted_iota(jnp.int32, (128, 128), 1)
+    )
+
+    def stat(phase, hop):
+        return remote(
+            stat_out.at[phase],
+            stat_in.at[phase, hop],
+            stat_send.at[phase, hop],
+            stat_recv.at[phase, hop],
+            tp=lax.rem(lane + hop, tp_count),
+        )
+
+    def share(phase, sums):
+        stat_out[phase] = jnp.zeros(stat_out.shape[1:], f32)
+        row = 0
+        for item in sums:
+            for group in range(groups):
+                part = item[group * 128 : (group + 1) * 128]
+                spread = jnp.where(eye, jnp.broadcast_to(part, (128, 128)), 0.0)
+                stat_out[phase, row : row + 1] = jnp.sum(spread, axis=0, keepdims=True)
+                row += 1
+        for hop in range(1, tp_count):
+            begin(stat(phase, hop))
+
+    def shared(phase):
+        value = stat_out[phase]
+        for hop in range(1, tp_count):
+            stat(phase, hop).wait_recv()
+            value += stat_in[phase, hop]
+        columns_of = []
+        for item in range(2):
+            parts = []
+            for group in range(groups):
+                row = item * groups + group
+                spread = jnp.broadcast_to(value[row : row + 1], (128, 128))
+                parts.append(jnp.sum(jnp.where(eye, spread, 0.0), axis=1, keepdims=True))
+            columns_of.append(jnp.concatenate(parts, axis=0))
+        return columns_of
+
+    saved_conv = saved_ref[...].astype(f32)
+    share(
+        0,
+        (
+            jnp.sum(saved_conv, axis=1, keepdims=True),
+            jnp.sum(saved_conv * saved_conv, axis=1, keepdims=True),
+        ),
+    )
+
     def pair_sum(step, hop):
         block = lax.rem(me + step, sp_count)
         column = lax.rem(lane + 2 * hop, tp_count)
-        return partial_ref[block, :, columns(column)].astype(jnp.float32) + pair_in[
-            step, hop
-        ].astype(jnp.float32)
+        return partial_ref[block, :, columns(column)].astype(f32) + pair_in[step, hop].astype(f32)
 
     lag = 2
     for at in range(sp_count + lag):
@@ -284,7 +355,7 @@
             step = order[at]
             for hop in range(1, chips):
                 swapped(step, hop).wait_recv()
-                side_out[step, hop - 1] = pair_sum(step, hop).astype(jnp.bfloat16)
+                side_out[step, hop - 1] = pair_sum(step, hop).astype(bf16)
                 begin(beside(step, hop))
         if at >= lag:
             step = order[at - lag]
@@ -292,43 +363,175 @@
             value = pair_sum(step, 0)
             for hop in range(1, chips):
                 beside(step, hop).wait_recv()
-                value += side_in[step, hop - 1].astype(jnp.float32)
+                value += side_in[step, hop - 1].astype(f32)
             if step:
-                total[step] = value.astype(jnp.bfloat16)
+                total[step] = value.astype(bf16)
                 begin(far(step))
             else:
-                out_ref[me] = value.astype(jnp.bfloat16)
+                returned[me] = value.astype(bf16)
+
+    total_sum, square_sum = shared(0)
+    mean_c = total_sum / conv_width
+    var_c = square_sum / conv_width - mean_c * mean_c
+    inv_std = lax.rsqrt(var_c + norm_eps)
+    normed = (saved_conv - mean_c) * inv_std
+    norm_sigmoid = jax.nn.sigmoid(normed)
+    mixed = (normed * norm_sigmoid).astype(bf16)
+
     for step in range(1, sp_count):
         far(step).wait_recv()
+    routed_sum = jnp.dot(
+        picks_ref[...],
+        returned[...].reshape(-1, width),
+        preferred_element_type=f32,
+    )
+    own_grad = (upstream_ref[...].astype(f32) + routed_sum).astype(bf16)
+    grad_stream_ref[...] = own_grad
+    full[:, columns(lane)] = own_grad
+
+    def spread_full(hop):
+        return remote(
+            full.at[:, columns(lane)],
+            full.at[:, columns(lane)],
+            full_send.at[0, hop],
+            full_recv.at[0, hop],
+            tp=lax.rem(lane + 2 * hop, tp_count),
+        )
+
+    def hand_over(hop):
+        column = lax.rem(lane + tp_count - 2 * hop, tp_count)
+        return remote(
+            full.at[:, columns(column)],
+            full.at[:, columns(column)],
+            full_send.at[1, hop],
+            full_recv.at[1, hop],
+            tp=partner,
+        )
+
+    for hop in range(1, chips):
+        begin(spread_full(hop))
+    begin(hand_over(0))
+    for hop in range(1, chips):
+        spread_full(hop).wait_recv()
+        begin(hand_over(hop))
+    for hop in range(chips):
+        hand_over(hop).wait_recv()
+
+    for column in range(tp_count):
+        block = contract_rows(full[:, column * width : (column + 1) * width], mixed)
+        per = sp_count // tp_count
+        parts_out[column * per : (column + 1) * per] = block.reshape(
+            per, width // per, channels
+        ).astype(bf16)
+
+    def give_parts(step):
+        to = lax.rem(me + step, sp_count)
+        return remote(
+            parts_out.at[to],
+            parts_in.at[step],
+            parts_send.at[step],
+            parts_recv.at[step],
+            sp=to,
+        )
+
+    for step in range(1, sp_count):
+        begin(give_parts(step))
+
+    grad_mixed = jnp.dot(full[...], proj_ref[...], preferred_element_type=f32)
+    grad_normed = grad_mixed * norm_sigmoid * (1.0 + normed * (1.0 - norm_sigmoid))
+    share(
+        1,
+        (
+            jnp.sum(grad_normed, axis=1, keepdims=True),
+            jnp.sum(grad_normed * normed, axis=1, keepdims=True),
+        ),
+    )
+    first_sum, second_sum = shared(1)
+    grad_conv = inv_std * (
+        grad_normed - first_sum / conv_width - normed * (second_sum / conv_width)
+    )
+    padded[:tok_count] = grad_conv
+    rim = rim_in.shape[0]
+    rim_copy = remote(
+        padded.at[pl.ds(0, rim)],
+        rim_in,
+        rim_send.at[0],
+        rim_recv.at[0],
+        sp=lax.rem(me + sp_count - 1, sp_count),
+    )
+    begin(rim_copy)
+    gate_sig = jax.nn.sigmoid(gate_ref[...].astype(f32))
+    rim_copy.wait_recv()
+    padded[tok_count:] = jnp.where(me == sp_count - 1, 0.0, rim_in[...])
+    grad_glu = jnp.zeros((tok_count, channels), f32)
+    for offset in range(taps_ref.shape[0]):
+        grad_glu += taps_ref[offset : offset + 1] * padded[offset : offset + tok_count]
+    grad_value_ref[...] = (grad_glu * gate_sig).astype(bf16)
+    grad_gate_ref[...] = (
+        grad_glu * value_ref[...].astype(f32) * gate_sig * (1.0 - gate_sig)
+    ).astype(bf16)
+
+    summed = parts_out[me].astype(f32)
+    for step in range(1, sp_count):
+        give_parts(step).wait_recv()
+        summed += parts_in[step].astype(f32)
+    grad_proj_ref[...] = summed
     for copy in started:
         copy.wait_send()
 
 
-def send_back(partial_rows, sp_count, tp_count):
+def finish(sp_count, tp_count, partial_rows, picks, upstream_own, *conv_args):
+    conv_saved, out_proj, conv_taps = conv_args[:3]
     blocks, capacity, model_width = partial_rows.shape
+    tok_count, channels = conv_saved.shape
     width = model_width // tp_count
     chips = tp_count // 2
+    rim = -(-(conv_taps.shape[0] - 1) // 8) * 8
     dma, vmem = pltpu.SemaphoreType.DMA, pltpu.VMEM
+    f32, bf16 = jnp.float32, jnp.bfloat16
+    proj_rows = model_width // sp_count
+    shape = jax.ShapeDtypeStruct
     return pl.pallas_call(
-        functools.partial(return_kernel, sp_count, tp_count),
-        out_shape=jax.ShapeDtypeStruct((blocks, capacity, width), jnp.bfloat16),
-        in_specs=[pl.BlockSpec(memory_space=vmem)],
-        out_specs=pl.BlockSpec(memory_space=vmem),
+        functools.partial(tail_kernel, sp_count, tp_count),
+        out_shape=(
+            shape((tok_count, width), bf16),
+            shape((tok_count, channels), bf16),
+            shape((tok_count, channels), bf16),
+            shape((proj_rows, channels), f32),
+        ),
+        in_specs=[pl.BlockSpec(memory_space=vmem)] * 8,
+        out_specs=[pl.BlockSpec(memory_space=vmem)] * 4,
         scratch_shapes=[
-            vmem((sp_count, chips, capacity, width), jnp.bfloat16),
-            vmem((sp_count, chips - 1, capacity, width), jnp.bfloat16),
-            vmem((sp_count, chips - 1, capacity, width), jnp.bfloat16),
-            vmem((sp_count, capacity, width), jnp.bfloat16),
+            vmem((sp_count, chips, capacity, width), bf16),
+            vmem((sp_count, chips - 1, capacity, width), bf16),
+            vmem((sp_count, chips - 1, capacity, width), bf16),
+            vmem((sp_count, capacity, width), bf16),
+            vmem((sp_count, capacity, width), bf16),
+            vmem((tok_count, model_width), bf16),
+            vmem((2, 8, 128), f32),
+            vmem((2, tp_count, 8, 128), f32),
+            vmem((sp_count, proj_rows, channels), bf16),
+            vmem((sp_count, proj_rows, channels), bf16),
+            vmem((rim, channels), f32),
+            vmem((tok_count + rim, channels), f32),
             dma((sp_count, chips)),
             dma((sp_count, chips)),
             dma((sp_count, chips - 1)),
             dma((sp_count, chips - 1)),
             dma((sp_count,)),
             dma((sp_count,)),
+            dma((2, chips)),
+            dma((2, chips)),
+            dma((2, tp_count)),
+            dma((2, tp_count)),
+            dma((sp_count,)),
+            dma((sp_count,)),
+            dma((1,)),
+            dma((1,)),
         ],
         compiler_params=pltpu.CompilerParams(collective_id=1, has_side_effects=True),
-        name="send_back",
-    )(partial_rows)
+        name="finish",
+    )(partial_rows, picks, upstream_own, *conv_args)
 
 
 def expert_backward(expert_rows, expert_cot, gate_weight, up_weight, down_weight):
@@ -398,54 +601,18 @@
     partial_rows = times_transposed(grad_gate_pre, gate_weight) + times_transposed(
         grad_up_pre, up_weight
     )
-    returned = send_back(
-        partial_rows.astype(jnp.bfloat16).reshape(expert_count, capacity, model_width),
+    grad_stream, grad_value, grad_gate, grad_out_proj = finish(
         expert_count,
         lax.axis_size("tp"),
-    )
-    routed_sum = contract_rows(picks, returned.reshape(expert_count * capacity, slice_width))
-    upstream_own = lax.dynamic_slice_in_dim(upstream, column_start, slice_width, 1)
-    grad_stream = (upstream_own.astype(jnp.float32) + routed_sum).astype(jnp.bfloat16)
-    full_grad = lax.all_gather(grad_stream, "tp", axis=1, tiled=True)
-    conv_width = conv_saved.shape[1] * lax.axis_size("tp")
-    saved_conv = conv_saved.astype(jnp.float32)
-    total_sum, square_sum = lax.psum(
-        (jnp.sum(saved_conv, axis=1), jnp.sum(saved_conv * saved_conv, axis=1)), "tp"
-    )
-    mean_c = (total_sum / conv_width)[:, None]
-    var_c = (square_sum / conv_width)[:, None] - mean_c * mean_c
-    inv_std = lax.rsqrt(var_c + norm_eps)
-    normed = (saved_conv - mean_c) * inv_std
-    norm_sigmoid = jax.nn.sigmoid(normed)
-    mixed = (normed * norm_sigmoid).astype(jnp.bfloat16)
-    grad_mixed = jnp.dot(full_grad, out_proj, preferred_element_type=jnp.float32)
-    grad_normed = grad_mixed * norm_sigmoid * (1.0 + normed * (1.0 - norm_sigmoid))
-    first_sum, second_sum = lax.psum(
-        (jnp.sum(grad_normed, axis=1), jnp.sum(grad_normed * normed, axis=1)), "tp"
-    )
-    grad_conv = inv_std * (
-        grad_normed - (first_sum / conv_width)[:, None] - normed * (second_sum / conv_width)[:, None]
-    )
-    kernel_width = conv_taps.shape[0]
-    rim_rows = passed_along(grad_conv[: kernel_width - 1], "sp", -1)
-    padded = jnp.concatenate([grad_conv, rim_rows], axis=0)
-    grad_glu = jnp.zeros_like(grad_conv)
-    for offset in range(kernel_width):
-        grad_glu = grad_glu + conv_taps[offset][None, :] * padded[offset : offset + tok_count]
-    gate_sig = jax.nn.sigmoid(glu_gate.astype(jnp.float32))
-    grad_value = (grad_glu * gate_sig).astype(jnp.bfloat16)
-    grad_gate = (grad_glu * glu_value.astype(jnp.float32) * gate_sig * (1.0 - gate_sig)).astype(
-        jnp.bfloat16
-    )
-    proj_parts = contract_rows(full_grad, mixed).astype(jnp.bfloat16)
-    proj_parts = lax.all_to_all(
-        proj_parts.reshape(expert_count, -1, mixed.shape[1]),
-        "sp",
-        split_axis=0,
-        concat_axis=0,
-        tiled=True,
-    )
-    grad_out_proj = jnp.sum(proj_parts.astype(jnp.float32), axis=0)
+        partial_rows.astype(jnp.bfloat16).reshape(expert_count, capacity, model_width),
+        picks.T,
+        upstream_part,
+        conv_saved,
+        out_proj,
+        conv_taps,
+        glu_value,
+        glu_gate,
+    )
     return (
         grad_stream,
         grad_value,

time: 206 us -> 182 us (0.88)
  the two profiles are of different devices: /device:TPU:0 before, /device:TPU:27 now
where the time goes in v3:
time: 182 us; the launch traced here: 181 us
  Pallas kernels  134 us (74%)
  matrix products  35.9 us (20%)
  local copies, waits for them, and re-layouts  8.8 us (5%)
    pallas_call x1, Pallas kernels, dispatch(): pl.pallas_call(functools.partial(dispatch_kernel, sp_count, tp_count), ou...  69.1 us
    pallas_call x1, Pallas kernels, finish(): pl.pallas_call(functools.partial(tail_kernel, sp_count, tp_count), out_sh...  65.4 us
    dot_general x3, matrix products, contract_rows(): lax.dot_general(left, right, (((0,), (0,)), ((), ())), preferred_element_...  13.9 us
    dot_general x3, matrix products, times_transposed(): lax.dot_general(left, right, (((1,), (1,)), ((), ())), preferred_element_...  10.3 us
    unnamed x16, local copies, waits for them, and re-layouts  6.22 us
    dot_general x1, matrix products, expert_backward(): up_pre = jnp.dot(expert_rows, up_weight, preferred_element_type=jnp.float32)  5.33 us

profile of v3, /device:TPU:27, one launch (start us, length us, event | category | flops | bytes accessed | tf_op | source)
XLA Modules:
  0.0 181.3 jit_solution(12313620134751769936)
XLA Ops:
  0.6 0.0 copy-start
  0.6 0.9 fusion.27
  1.5 0.2 select_reduce_fusion.1
  1.7 0.8 fusion.26
  2.5 0.3 add_reduce_fusion
  2.8 1.0 constant_dynamic-slice_fusion.upstream_ref
  3.8 0.0 copy-start.1
  3.8 1.4 multiply_convert_fusion.1
  5.2 2.4 %convolution_convert_fusion = bf16[1024,512]{1,0:T(8,128)(2,1)} fusion(s32[256]{0:T(256)S(1)} %get-tuple-element.27, s32[256]{0:T(256)S(1)} %get-tuple-element.28, bf16[256,2048]{1,0:T(8,128)(2,1)} %param.13, s32[]{:T(128)S(6)} %select_n.18), kind=kOutput, calls=%fused_computation.20 | convolution fusion | flops 270532608 | bytes 1312772 | tf_op jit(solution)/shard_map/dot_general | solution.py:582
  7.6 69.1 %dispatch.1 = (bf16[8,128,2048]{2,1,0:T(8,128)(2,1)}, bf16[8,128,2048]{2,1,0:T(8,128)(2,1)}) custom-call(bf16[8,128,512]{2,1,0:T(8,128)(2,1)} %bitcast.43, bf16[8,128,512]{2,1,0:T(8,128)(2,1)} %bitcast.42), custom_call_target="tpu_custom_call" | custom-call | tf_op jit(solution)/shard_map/dispatch/pallas_call | solution.py:188
  76.7 0.0 copy-done.1
  76.7 0.0 copy-start.2
  76.7 5.3 %fusion.1 = f32[1024,512]{1,0:T(8,128)S(1)} fusion(bf16[1024,2048]{1,0:T(8,128)(2,1)} %bitcast.50, bf16[1,2048,512]{2,1,0:T(8,128)(2,1)} %param.22), kind=kOutput, calls=%fused_computation.5 | convolution fusion | flops 2147483648 | bytes 8388608 | tf_op jit(solution)/shard_map/dot_general | solution.py:539
  82.0 0.0 copy-done
  82.0 0.0 copy-done.2
  82.1 0.0 copy-start.3
  82.1 2.3 %fusion.7 = f32[1024,512]{1,0:T(8,128)S(1)} fusion(bf16[1024,2048]{1,0:T(8,128)(2,1)S(1)} %bitcast.51, bf16[1,2048,512]{2,1,0:T(8,128)(2,1)S(1)} %copy-done), kind=kOutput, calls=%fused_computation.11 | convolution fusion | flops 2147483648 | bytes 8388608 | tf_op jit(solution)/shard_map/dot_general | solution.py:538
  84.4 0.0 copy-done.3
  84.4 0.0 copy-start.4
  84.4 4.8 %convolution_bitcast_fusion = f32[1,512,2048]{2,1,0:T(8,128)} fusion(bf16[1024,2048]{1,0:T(8,128)(2,1)S(1)} %bitcast.54, f32[1024,512]{1,0:T(8,128)S(1)} %fusion.7, f32[1024,512]{1,0:T(8,128)S(1)} %fusion.1), kind=kOutput, calls=%fused_computation.1 | convolution fusion | flops 2152726528 | bytes 12582912 | tf_op jit(solution)/shard_map/dot_general | solution.py:17
  89.2 0.0 copy-done.4
  89.2 3.6 %select_convert_fusion = (bf16[1024,512]{1,0:T(8,128)(2,1)S(1)}, bf16[1024,512]{1,0:T(8,128)(2,1)S(1)}) fusion(f32[1024,512]{1,0:T(8,128)S(1)} %fusion.1, f32[1024,512]{1,0:T(8,128)S(1)} %fusion.7, bf16[1024,2048]{1,0:T(8,128)(2,1)S(1)} %bitcast.55, bf16[1,512,2048]{2,1,0:T(8,128)(2,1)S(1)} %copy-done.4), kind=kOutput, calls=%fused_computation.14 | convolution fusion | flops 2159017984 | bytes 12582912 | tf_op jit(solution)/shard_map/dot_general | solution.py:23
  92.8 4.7 %convolution_bitcast_fusion.1 = f32[1,2048,512]{2,1,0:T(8,128)} fusion(bf16[1024,2048]{1,0:T(8,128)(2,1)S(1)} %bitcast.52, bf16[1024,512]{1,0:T(8,128)(2,1)S(1)} %get-tuple-element.21), kind=kOutput, calls=%fused_computation.2 | convolution fusion | flops 2147483648 | bytes 9437184 | tf_op jit(solution)/shard_map/dot_general | solution.py:17
  97.5 4.5 %convolution_bitcast_fusion.2 = f32[1,2048,512]{2,1,0:T(8,128)} fusion(bf16[1024,2048]{1,0:T(8,128)(2,1)S(1)} %bitcast.53, bf16[1024,512]{1,0:T(8,128)(2,1)S(1)} %get-tuple-element.22), kind=kOutput, calls=%fused_computation.3 | convolution fusion | flops 2147483648 | bytes 9437184 | tf_op jit(solution)/shard_map/dot_general | solution.py:17
  102.0 0.0 copy-start.5
  102.0 2.4 %fusion.5 = f32[1024,2048]{1,0:T(8,128)S(1)} fusion(bf16[1024,512]{1,0:T(8,128)(2,1)S(1)} %get-tuple-element.22, bf16[1,2048,512]{2,1,0:T(8,128)(2,1)S(1)} %copy-done), kind=kOutput, calls=%fused_computation.9 | convolution fusion | flops 2147483648 | bytes 11534336 | tf_op jit(solution)/shard_map/dot_general | solution.py:23
  104.3 0.0 copy-done.5
  104.4 4.3 %add_convert_fusion = bf16[1024,2048]{1,0:T(8,128)(2,1)} fusion(f32[1024,2048]{1,0:T(8,128)S(1)} %fusion.5, bf16[1024,512]{1,0:T(8,128)(2,1)S(1)} %get-tuple-element.21, bf16[1,2048,512]{2,1,0:T(8,128)(2,1)S(1)} %copy-done.5), kind=kOutput, calls=%fused_computation | convolution fusion | flops 2151677952 | bytes 15728640 | tf_op jit(solution)/shard_map/dot_general | solution.py:23
  108.7 1.1 add_convert_fusion.1.picks_ref
  109.7 65.4 %finish.1 = (bf16[256,512]{1,0:T(8,128)(2,1)}, bf16[256,128]{1,0:T(8,128)(2,1)}, bf16[256,128]{1,0:T(8,128)(2,1)}, f32[256,128]{1,0:T(8,128)}) custom-call(bf16[8,128,2048]{2,1,0:T(8,128)(2,1)} %bitcast.41, bf16[256,1024]{1,0:T(8,128)(2,1)} %add_convert_fusion.1.picks_ref, bf16[256,512]{1,0:T(8,128)(2,1)} %copy-done.1, bf16[256,128]{1,0:T(8,128)(2,1)} %saved_ref.1, ...), custom_call_target="tpu_custom_call" | custom-call | tf_op jit(solution)/shard_map/finish/pallas_call | solution.py:494
  175.1 1.7 copy.23
  176.8 1.5 copy.24
  178.2 1.5 copy.25
  179.7 1.6 copy.26
  (1 shorter events, 0.0 us)
Async XLA Ops:
  0.6 81.4 %copy-start = (bf16[1,2048,512]{2,1,0:T(8,128)(2,1)S(1)}, bf16[1,2048,512]{2,1,0:T(8,128)(2,1)}, u32[]{:S(2)}) copy-start(bf16[1,2048,512]{2,1,0:T(8,128)(2,1)} %param.21) | copy-start | bytes 6291460
  3.8 72.9 %copy-start.1 = (bf16[256,512]{1,0:T(8,128)(2,1)}, bf16[256,512]{1,0:T(8,128)(2,1)S(1)}, u32[]{:S(2)}) copy-start(bf16[256,512]{1,0:T(8,128)(2,1)S(1)} %constant_dynamic-slice_fusion.upstream_ref) | copy-start | bytes 786436
  76.7 5.4 %copy-start.2 = (bf16[8,128,2048]{2,1,0:T(8,128)(2,1)S(1)}, bf16[8,128,2048]{2,1,0:T(8,128)(2,1)}, u32[]{:S(2)}) copy-start(bf16[8,128,2048]{2,1,0:T(8,128)(2,1)} %get-tuple-element.13) | copy-start | bytes 12582916
  82.1 2.3 %copy-start.3 = (bf16[8,128,2048]{2,1,0:T(8,128)(2,1)S(1)}, bf16[8,128,2048]{2,1,0:T(8,128)(2,1)}, u32[]{:S(2)}) copy-start(bf16[8,128,2048]{2,1,0:T(8,128)(2,1)} %get-tuple-element.14) | copy-start | bytes 12582916
  84.4 4.8 %copy-start.4 = (bf16[1,512,2048]{2,1,0:T(8,128)(2,1)S(1)}, bf16[1,512,2048]{2,1,0:T(8,128)(2,1)}, u32[]{:S(2)}) copy-start(bf16[1,512,2048]{2,1,0:T(8,128)(2,1)} %param.23) | copy-start | bytes 6291460
  102.0 2.4 %copy-start.5 = (bf16[1,2048,512]{2,1,0:T(8,128)(2,1)S(1)}, bf16[1,2048,512]{2,1,0:T(8,128)(2,1)}, u32[]{:S(2)}) copy-start(bf16[1,2048,512]{2,1,0:T(8,128)(2,1)} %param.22) | copy-start | bytes 6291460

commit v4 on v3

--- a/solution.py
+++ b/solution.py
@@ -83,6 +83,8 @@
     tp_count,
     rows_ref,
     cot_ref,
+    own_rows_ref,
+    own_cot_ref,
     got_rows,
     got_cot,
     far_send,
@@ -116,9 +118,8 @@
 
     def beside(which, step, hop):
         block = lax.rem(me + sp_count - step, sp_count)
-        source = sources[which].at[me] if step == 0 else place(which, block, lane)
-        return remote(
-            source,
+        return remote(
+            place(which, block, lane),
             place(which, block, lane),
             side_send.at[which, step, hop],
             side_recv.at[which, step, hop],
@@ -128,11 +129,8 @@
     def paired(which, step, hop):
         block = lax.rem(me + sp_count - step, sp_count)
         column = lax.rem(lane + tp_count - 2 * hop, tp_count)
-        source = (
-            sources[which].at[me] if step == 0 and hop == 0 else place(which, block, column)
-        )
-        return remote(
-            source,
+        return remote(
+            place(which, block, column),
             place(which, block, column),
             pair_send.at[which, step, hop],
             pair_recv.at[which, step, hop],
@@ -145,10 +143,9 @@
         copy.start()
         started.append(copy)
 
-    order = [(which, step) for which in range(2) for step in range(1, sp_count)]
     own = [
-        pltpu.make_async_copy(sources[which].at[me], place(which, me, lane), own_sem.at[which])
-        for which in range(2)
+        pltpu.make_async_copy(own_rows_ref, got_rows.at[me], own_sem.at[0]),
+        pltpu.make_async_copy(own_cot_ref, got_cot.at[me], own_sem.at[1]),
     ]
     for which in range(2):
         own[which].start()
@@ -156,13 +153,12 @@
             begin(far(which, step))
     arrivals = []
     for which in range(2):
-        arrivals += [(which, step) for step in range(sp_count)]
+        arrivals += [(which, step) for step in range(1, sp_count)]
     lag = 2
     for at in range(len(arrivals) + lag):
         if at < len(arrivals):
             which, step = arrivals[at]
-            if step:
-                far(which, step).wait_recv()
+            far(which, step).wait_recv()
             for hop in range(1, chips):
                 begin(beside(which, step, hop))
             begin(paired(which, step, 0))
@@ -180,7 +176,7 @@
         copy.wait()
 
 
-def dispatch(send_rows, send_cot, sp_count, tp_count):
+def dispatch(send_rows, send_cot, own_rows, own_cot, sp_count, tp_count):
     blocks, capacity, width = send_rows.shape
     full = jax.ShapeDtypeStruct((blocks, capacity, width * tp_count), send_rows.dtype)
     dma = pltpu.SemaphoreType.DMA
@@ -188,14 +184,14 @@
     return pl.pallas_call(
         functools.partial(dispatch_kernel, sp_count, tp_count),
         out_shape=(full, full),
-        in_specs=[pl.BlockSpec(memory_space=pltpu.VMEM)] * 2,
+        in_specs=[pl.BlockSpec(memory_space=pltpu.VMEM)] * 4,
         out_specs=[pl.BlockSpec(memory_space=pl.ANY)] * 2,
         scratch_shapes=[dma((2, sp_count))] * 2
         + [dma((2, sp_count, chips))] * 4
         + [dma((2,))],
         compiler_params=pltpu.CompilerParams(collective_id=0, has_side_effects=True),
         name="dispatch",
-    )(send_rows, send_cot)
+    )(send_rows, send_cot, own_rows, own_cot)
 
 
 def tail_kernel(
@@ -583,10 +579,19 @@
     send_cot = (
         row_weights[:, None] * jnp.dot(picks, upstream_part, preferred_element_type=jnp.float32)
     ).astype(jnp.bfloat16)
+    own_start = lax.axis_index("sp") * capacity
+    own_picks = lax.dynamic_slice_in_dim(picks, own_start, capacity, 0)
+    own_weights = lax.dynamic_slice_in_dim(row_weights, own_start, capacity, 0)
+    own_rows = jnp.dot(own_picks, stream, preferred_element_type=jnp.float32).astype(jnp.bfloat16)
+    own_cot = (
+        own_weights[:, None] * jnp.dot(own_picks, upstream, preferred_element_type=jnp.float32)
+    ).astype(jnp.bfloat16)
     part_shape = (expert_count, capacity, slice_width)
     got_rows, got_cot = dispatch(
         send_rows.reshape(part_shape),
         send_cot.reshape(part_shape),
+        own_rows,
+        own_cot,
         expert_count,
         lax.axis_size("tp"),
     )

time: 182 us -> 184 us (1.011)
  matrix products: 35.9 us -> 39.4 us
  Pallas kernels: 134 us -> 132 us
    dot_general x0 -> x2, matrix products: none -> 4.44 us  [the longest x1 2.5 us: on_device(): jnp.dot(own_picks, upstream, preferred_element_type=jnp.float32)]
    unnamed x16 -> x18, local copies, waits for them, and re-layouts: 6.22 us -> 6.22 us
where the time goes in v4:
time: 184 us; the launch traced here: 183 us
  Pallas kernels  132 us (72%)
  matrix products  39.4 us (21%)
  local copies, waits for them, and re-layouts  8.87 us (5%)
  other arithmetic  2.19 us (1%)
    pallas_call x1, Pallas kernels, dispatch(): pl.pallas_call(functools.partial(dispatch_kernel, sp_count, tp_count), ou...  68 us
    pallas_call x1, Pallas kernels, finish(): pl.pallas_call(functools.partial(tail_kernel, sp_count, tp_count), out_sh...  63.9 us
    dot_general x3, matrix products, contract_rows(): lax.dot_general(left, right, (((0,), (0,)), ((), ())), preferred_element_...  13.9 us
    dot_general x3, matrix products, times_transposed(): lax.dot_general(left, right, (((1,), (1,)), ((), ())), preferred_element_...  10.3 us
    unnamed x18, local copies, waits for them, and re-layouts  6.22 us
    dot_general x1, matrix products, expert_backward(): up_pre = jnp.dot(expert_rows, up_weight, preferred_element_type=jnp.float32)  5.32 us

profile of v4, /device:TPU:27, one launch (start us, length us, event | category | flops | bytes accessed | tf_op | source)
XLA Modules:
  0.0 183.1 jit_solution(10025574881405162794)
XLA Ops:
  0.6 0.0 copy-start
  0.6 0.9 fusion.28
  1.5 0.2 select_reduce_fusion.1
  1.7 0.8 fusion.27
  2.5 1.1 add_convert_fusion.2
  3.6 0.1 dynamic_slice.15
  3.7 0.0 copy-start.2
  3.7 2.5 %fusion.own_cot_ref = bf16[128,2048]{1,0:T(8,128)(2,1)} fusion(bf16[256,2048]{1,0:T(8,128)(2,1)} %param.12, f32[128]{0:T(128)S(1)} %dynamic_slice.15, bf16[1024,256]{1,0:T(8,128)(2,1)} %get-tuple-element.23, s32[]{:T(128)S(6)} %select_n.25), kind=kOutput, calls=%fused_computation.5 | convolution fusion | flops 134742016 | bytes 1638916 | tf_op jit(solution)/shard_map/dot_general | solution.py:587
  6.2 1.0 constant_dynamic-slice_fusion.upstream_ref
  7.2 0.0 copy-start.1
  7.2 1.4 multiply_convert_fusion.1
  8.6 0.0 copy-done.2
  8.6 1.9 %convolution_convert_fusion.own_rows_ref = bf16[128,2048]{1,0:T(8,128)(2,1)} fusion(bf16[256,2048]{1,0:T(8,128)(2,1)S(1)} %copy-done.2, bf16[1024,256]{1,0:T(8,128)(2,1)} %get-tuple-element.23, s32[]{:T(128)S(6)} %select_n.25), kind=kOutput, calls=%fused_computation.6 | convolution fusion | flops 134479872 | bytes 1638404 | tf_op jit(solution)/shard_map/dot_general | solution.py:585
  10.6 1.4 convolution_convert_fusion.1
  12.0 0.0 copy-done.1
  12.0 68.0 %dispatch.1 = (bf16[8,128,2048]{2,1,0:T(8,128)(2,1)}, bf16[8,128,2048]{2,1,0:T(8,128)(2,1)}) custom-call(bf16[8,128,512]{2,1,0:T(8,128)(2,1)} %bitcast.45, bf16[8,128,512]{2,1,0:T(8,128)(2,1)} %bitcast.44, bf16[128,2048]{1,0:T(8,128)(2,1)} %convolution_convert_fusion.own_rows_ref, bf16[128,2048]{1,0:T(8,128)(2,1)} %fusion.own_cot_ref), custom_call_target="tpu_custom_call" | custom-call | tf_op jit(solution)/shard_map/dispatch/pallas_call | solution.py:184
  80.0 0.0 copy-start.3
  80.0 5.3 %fusion.2 = f32[1024,512]{1,0:T(8,128)S(1)} fusion(bf16[1024,2048]{1,0:T(8,128)(2,1)} %bitcast.52, bf16[1,2048,512]{2,1,0:T(8,128)(2,1)} %param.22), kind=kOutput, calls=%fused_computation.8 | convolution fusion | flops 2147483648 | bytes 8388608 | tf_op jit(solution)/shard_map/dot_general | solution.py:535
  85.3 0.0 copy-done
  85.3 0.0 copy-done.3
  85.3 0.0 copy-start.4
  85.3 2.3 %fusion.8 = f32[1024,512]{1,0:T(8,128)S(1)} fusion(bf16[1024,2048]{1,0:T(8,128)(2,1)S(1)} %bitcast.53, bf16[1,2048,512]{2,1,0:T(8,128)(2,1)S(1)} %copy-done), kind=kOutput, calls=%fused_computation.14 | convolution fusion | flops 2147483648 | bytes 8388608 | tf_op jit(solution)/shard_map/dot_general | solution.py:534
  87.7 0.0 copy-done.4
  87.7 0.0 copy-start.5
  87.7 4.8 %convolution_bitcast_fusion = f32[1,512,2048]{2,1,0:T(8,128)} fusion(bf16[1024,2048]{1,0:T(8,128)(2,1)S(1)} %bitcast.56, f32[1024,512]{1,0:T(8,128)S(1)} %fusion.8, f32[1024,512]{1,0:T(8,128)S(1)} %fusion.2), kind=kOutput, calls=%fused_computation.1 | convolution fusion | flops 2152726528 | bytes 12582912 | tf_op jit(solution)/shard_map/dot_general | solution.py:17
  92.5 0.0 copy-done.5
  92.5 3.6 %select_convert_fusion = (bf16[1024,512]{1,0:T(8,128)(2,1)S(1)}, bf16[1024,512]{1,0:T(8,128)(2,1)S(1)}) fusion(f32[1024,512]{1,0:T(8,128)S(1)} %fusion.2, f32[1024,512]{1,0:T(8,128)S(1)} %fusion.8, bf16[1024,2048]{1,0:T(8,128)(2,1)S(1)} %bitcast.57, bf16[1,512,2048]{2,1,0:T(8,128)(2,1)S(1)} %copy-done.5), kind=kOutput, calls=%fused_computation.17 | convolution fusion | flops 2159017984 | bytes 12582912 | tf_op jit(solution)/shard_map/dot_general | solution.py:23
  96.1 4.7 %convolution_bitcast_fusion.1 = f32[1,2048,512]{2,1,0:T(8,128)} fusion(bf16[1024,2048]{1,0:T(8,128)(2,1)S(1)} %bitcast.54, bf16[1024,512]{1,0:T(8,128)(2,1)S(1)} %get-tuple-element.21), kind=kOutput, calls=%fused_computation.2 | convolution fusion | flops 2147483648 | bytes 9437184 | tf_op jit(solution)/shard_map/dot_general | solution.py:17
  100.8 4.5 %convolution_bitcast_fusion.2 = f32[1,2048,512]{2,1,0:T(8,128)} fusion(bf16[1024,2048]{1,0:T(8,128)(2,1)S(1)} %bitcast.55, bf16[1024,512]{1,0:T(8,128)(2,1)S(1)} %get-tuple-element.22), kind=kOutput, calls=%fused_computation.3 | convolution fusion | flops 2147483648 | bytes 9437184 | tf_op jit(solution)/shard_map/dot_general | solution.py:17
  105.2 0.0 copy-start.6
  105.2 2.4 %fusion.6 = f32[1024,2048]{1,0:T(8,128)S(1)} fusion(bf16[1024,512]{1,0:T(8,128)(2,1)S(1)} %get-tuple-element.22, bf16[1,2048,512]{2,1,0:T(8,128)(2,1)S(1)} %copy-done), kind=kOutput, calls=%fused_computation.12 | convolution fusion | flops 2147483648 | bytes 11534336 | tf_op jit(solution)/shard_map/dot_general | solution.py:23
  107.6 0.0 copy-done.6
  107.6 4.3 %add_convert_fusion = bf16[1024,2048]{1,0:T(8,128)(2,1)} fusion(f32[1024,2048]{1,0:T(8,128)S(1)} %fusion.6, bf16[1024,512]{1,0:T(8,128)(2,1)S(1)} %get-tuple-element.21, bf16[1,2048,512]{2,1,0:T(8,128)(2,1)S(1)} %copy-done.6), kind=kOutput, calls=%fused_computation | convolution fusion | flops 2151677952 | bytes 15728640 | tf_op jit(solution)/shard_map/dot_general | solution.py:23
  111.9 1.1 add_convert_fusion.1.picks_ref
  113.0 63.9 %finish.1 = (bf16[256,512]{1,0:T(8,128)(2,1)}, bf16[256,128]{1,0:T(8,128)(2,1)}, bf16[256,128]{1,0:T(8,128)(2,1)}, f32[256,128]{1,0:T(8,128)}) custom-call(bf16[8,128,2048]{2,1,0:T(8,128)(2,1)} %bitcast.43, bf16[256,1024]{1,0:T(8,128)(2,1)} %add_convert_fusion.1.picks_ref, bf16[256,512]{1,0:T(8,128)(2,1)} %copy-done.1, bf16[256,128]{1,0:T(8,128)(2,1)} %saved_ref.1, ...), custom_call_target="tpu_custom_call" | custom-call | tf_op jit(solution)/shard_map/finish/pallas_call | solution.py:490
  176.9 1.7 copy.23
  178.6 1.5 copy.24
  180.1 1.5 copy.25
  181.6 1.6 copy.26
  (1 shorter events, 0.0 us)
Async XLA Ops:
  0.6 84.7 %copy-start = (bf16[1,2048,512]{2,1,0:T(8,128)(2,1)S(1)}, bf16[1,2048,512]{2,1,0:T(8,128)(2,1)}, u32[]{:S(2)}) copy-start(bf16[1,2048,512]{2,1,0:T(8,128)(2,1)} %param.21) | copy-start | bytes 6291460
  3.7 4.9 %copy-start.2 = (bf16[256,2048]{1,0:T(8,128)(2,1)S(1)}, bf16[256,2048]{1,0:T(8,128)(2,1)}, u32[]{:S(2)}) copy-start(bf16[256,2048]{1,0:T(8,128)(2,1)} %param.13) | copy-start | bytes 3145732
  7.2 4.8 %copy-start.1 = (bf16[256,512]{1,0:T(8,128)(2,1)}, bf16[256,512]{1,0:T(8,128)(2,1)S(1)}, u32[]{:S(2)}) copy-start(bf16[256,512]{1,0:T(8,128)(2,1)S(1)} %constant_dynamic-slice_fusion.upstream_ref) | copy-start | bytes 786436
  80.0 5.3 %copy-start.3 = (bf16[8,128,2048]{2,1,0:T(8,128)(2,1)S(1)}, bf16[8,128,2048]{2,1,0:T(8,128)(2,1)}, u32[]{:S(2)}) copy-start(bf16[8,128,2048]{2,1,0:T(8,128)(2,1)} %get-tuple-element.13) | copy-start | bytes 12582916
  85.3 2.3 %copy-start.4 = (bf16[8,128,2048]{2,1,0:T(8,128)(2,1)S(1)}, bf16[8,128,2048]{2,1,0:T(8,128)(2,1)}, u32[]{:S(2)}) copy-start(bf16[8,128,2048]{2,1,0:T(8,128)(2,1)} %get-tuple-element.14) | copy-start | bytes 12582916
  87.7 4.8 %copy-start.5 = (bf16[1,512,2048]{2,1,0:T(8,128)(2,1)S(1)}, bf16[1,512,2048]{2,1,0:T(8,128)(2,1)}, u32[]{:S(2)}) copy-start(bf16[1,512,2048]{2,1,0:T(8,128)(2,1)} %param.23) | copy-start | bytes 6291460
  105.2 2.4 %copy-start.6 = (bf16[1,2048,512]{2,1,0:T(8,128)(2,1)S(1)}, bf16[1,2048,512]{2,1,0:T(8,128)(2,1)}, u32[]{:S(2)}) copy-start(bf16[1,2048,512]{2,1,0:T(8,128)(2,1)} %param.22) | copy-start | bytes 6291460
